TPU v7x, 256 devices: a whole 4x4x8 slice. The times are simulated.
256 devices in a mesh: sp: 64 (over z, y, core), tp: 4 (over x).
Axes of the slice: x: 4, y: 4, z: 8, core: 2. Of those that a mesh axis runs over, the one named last changes fastest.
Arguments:
- queries: bfloat16 [32768, 1024], P('sp', 'tp'), may hold values from -60 to 60
- keys: bfloat16 [32768, 1024], P('sp', 'tp'), may hold values from -6 to 6
- values: bfloat16 [32768, 1024], P('sp', 'tp'), may hold values from -6 to 6
- lambdas: float32 [8], P('tp'), may hold values from 0.3 to 0.8
- head_gain: float32 [128], replicated, may hold values from 0.1 to 1.9
- w_out: bfloat16 [1024, 2048], replicated, may hold values from -0.1875 to 0.1875
- residual_in: bfloat16 [32768, 2048], P(('sp', 'tp')), may hold values from -6 to 6
- norm_gain: float32 [2048], replicated, may hold values from 0.1 to 1.9
- route_ids: int32 [32768, 2], P(('sp', 'tp')), may hold values from 0 to 63, as said below
- route_weight: float32 [32768, 2], P(('sp', 'tp')), may hold values from 0.2 to 1
- w_gate: bfloat16 [64, 2048, 1024], P('sp', None, 'tp'), may hold values from -0.125 to 0.125
- w_up: bfloat16 [64, 2048, 1024], P('sp', None, 'tp'), may hold values from -0.125 to 0.125
- w_down: bfloat16 [64, 2048, 1024], P('sp', None, 'tp'), may hold values from -0.1875 to 0.1875
Outputs:
- layer_out: bfloat16 [32768, 2048], P(('sp', 'tp'))
Inputs may be any that keep to these rules, and one draw needn't show every extreme that they name: `route_ids`: each row names two different experts of one group (the same expert // 8). Among the 128 rows of one device (aligned blocks), no expert is named more than 8 times, and in every draw one expert is named exactly 8 times in the rows of every device.
All inputs are finite; a program needn't handle non-finite values.
Results may differ from a plain program's by a relative error of at most 0.015.
Values may be sent and summed in bfloat16 or wider, within the bound.
A program may use at most 128 MiB of HBM per device.

v0:
```python
import jax
import jax.numpy as jnp
from jax import lax
from jax.sharding import PartitionSpec as P

EPSILON = 1e-06
OUT_SCALE = 0.8
FLOOR_SCORE = -1e30


def swapped(value, axis, distance):
    mask = 2**distance
    pairs = [(source, source ^ mask) for source in range(lax.axis_size(axis))]
    return lax.ppermute(value, axis, pairs)


def block_length(total_rows):
    largest = 1
    for divisor in range(1, min(total_rows, 1024) + 1):
        if total_rows % divisor == 0:
            largest = divisor
    return largest


def slot_numbers(flat_ids):
    count_ids = flat_ids.shape[0]
    positions = lax.broadcasted_iota(jnp.int32, (count_ids, count_ids), 0)
    earlier = lax.broadcasted_iota(jnp.int32, (count_ids, count_ids), 1) < positions
    matches = (flat_ids[:, None] == flat_ids[None, :]) & earlier
    return jnp.sum(matches.astype(jnp.int32), axis=1)


def expert_hidden(arrived, gate_weight, up_weight):
    gate_proj = jnp.einsum(
        "secd,edf->secf", arrived, gate_weight, preferred_element_type=jnp.float32
    )
    up_proj = jnp.einsum("secd,edf->secf", arrived, up_weight, preferred_element_type=jnp.float32)
    return (jax.nn.silu(gate_proj) * up_proj).astype(jnp.bfloat16)


def send_back(results):
    return lax.all_to_all(results, "sp", split_axis=0, concat_axis=0, tiled=True)


def local(
    queries,
    keys,
    values,
    lambdas,
    head_gain,
    w_out,
    residual_in,
    norm_gain,
    route_ids,
    route_weight,
    w_gate,
    w_up,
    w_down,
):
    tok_rows = queries.shape[0]
    local_heads = lambdas.shape[0]
    head_dim = queries.shape[1] // (2 * local_heads)
    value_dim = 2 * head_dim
    score_scale = head_dim ** (-0.5)
    query_view = queries.reshape(tok_rows, local_heads, 2, head_dim)

    def absorb(running, key_piece, value_piece):
        key_count = key_piece.shape[0]
        step_rows = block_length(key_count)
        key_blocks = key_piece.reshape(key_count // step_rows, step_rows, local_heads, 2, head_dim)
        value_blocks = value_piece.reshape(
            key_count // step_rows, step_rows, local_heads, value_dim
        )

        def one_block(state, block_pair):
            key_block, value_block = block_pair
            running_max, running_sum, running_acc = state
            scores = (
                jnp.einsum(
                    "qhmd,khmd->hmqk", query_view, key_block, preferred_element_type=jnp.float32
                )
                * score_scale
            )
            new_max = jnp.maximum(running_max, jnp.max(scores, axis=-1))
            weights = jnp.exp(scores - new_max[..., None])
            shrink = jnp.exp(running_max - new_max)
            new_sum = running_sum * shrink + jnp.sum(weights, axis=-1)
            product = jnp.einsum(
                "hmqk,khv->hmqv",
                weights.astype(jnp.bfloat16),
                value_block,
                preferred_element_type=jnp.float32,
            )
            return ((new_max, new_sum, running_acc * shrink[..., None] + product), None)

        final_state, unused = lax.scan(one_block, running, (key_blocks, value_blocks))
        return final_state

    initial = (
        jnp.full((local_heads, 2, tok_rows), FLOOR_SCORE, jnp.float32),
        jnp.zeros((local_heads, 2, tok_rows), jnp.float32),
        jnp.zeros((local_heads, 2, tok_rows, value_dim), jnp.float32),
    )
    seq_bits = min(4, lax.axis_size("sp").bit_length() - 1)
    held_keys, held_values = (keys, values)
    state = absorb(initial, held_keys, held_values)
    for bit_number in range(seq_bits):
        came_keys, came_values = swapped((held_keys, held_values), "sp", bit_number)
        state = absorb(state, came_keys, came_values)
        if bit_number + 1 < seq_bits:
            held_keys = jnp.concatenate([held_keys, came_keys], axis=0)
            held_values = jnp.concatenate([held_values, came_values], axis=0)
    peaks, totals, numerators = state
    heads_out = numerators / totals[..., None]
    combined = heads_out[:, 0] - lambdas[:, None, None] * heads_out[:, 1]
    mean_square = jnp.mean(combined * combined, axis=-1, keepdims=True)
    normalized = combined * lax.rsqrt(mean_square + EPSILON) * head_gain * OUT_SCALE
    attended = (
        jnp.transpose(normalized, (1, 0, 2))
        .reshape(tok_rows, local_heads * value_dim)
        .astype(jnp.bfloat16)
    )
    dev_rows = residual_in.shape[0]
    token_rows = lax.all_to_all(attended, "tp", split_axis=0, concat_axis=1, tiled=True)
    mixed_sum = jnp.dot(token_rows, w_out, preferred_element_type=jnp.float32)
    mixed_out = mixed_sum.astype(jnp.bfloat16)
    carried = (residual_in.astype(jnp.float32) + mixed_out.astype(jnp.float32)).astype(jnp.bfloat16)
    carried_wide = carried.astype(jnp.float32)
    normed = (
        carried_wide
        * lax.rsqrt(jnp.mean(carried_wide * carried_wide, axis=-1, keepdims=True) + EPSILON)
        * norm_gain
    ).astype(jnp.bfloat16)
    model_width = normed.shape[1]
    experts_here = w_gate.shape[0]
    expert_count = experts_here * lax.axis_size("sp")
    capacity = max(2, 4 * dev_rows // expert_count)
    flat_ids = route_ids.reshape(-1)
    targets = flat_ids * capacity + slot_numbers(flat_ids)
    slot_ids = lax.broadcasted_iota(jnp.int32, (expert_count * capacity, dev_rows, 2), 0)
    placement_matrix = jnp.sum(
        (targets.reshape(1, dev_rows, 2) == slot_ids).astype(jnp.int32), axis=2
    ).astype(jnp.bfloat16)
    outgoing = jnp.dot(placement_matrix, normed, preferred_element_type=jnp.float32).astype(
        jnp.bfloat16
    )
    outgoing = outgoing.reshape(lax.axis_size("sp"), experts_here, capacity, model_width)
    full_gate, full_up, full_down = (
        lax.all_gather(w_gate, "tp", axis=2, tiled=True),
        lax.all_gather(w_up, "tp", axis=2, tiled=True),
        lax.all_gather(w_down, "tp", axis=2, tiled=True),
    )
    hidden_units = expert_hidden(
        lax.all_to_all(outgoing, "sp", split_axis=0, concat_axis=0, tiled=True), full_gate, full_up
    )
    summed = jnp.einsum(
        "secf,edf->secd", hidden_units, full_down, preferred_element_type=jnp.float32
    )
    returned = send_back(summed.astype(jnp.bfloat16))
    flat_back = returned.reshape(expert_count * capacity, model_width)
    picked = (
        jnp.take(flat_back, targets, axis=0).astype(jnp.float32).reshape(dev_rows, 2, model_width)
    )
    layer_out = carried_wide + jnp.sum(route_weight[..., None] * picked, axis=1)
    return layer_out.astype(jnp.bfloat16)


def solution(mesh):
    placed = (
        P("sp", "tp"),
        P("sp", "tp"),
        P("sp", "tp"),
        P("tp"),
        P(),
        P(),
        P(("sp", "tp"), None),
        P(),
        P(("sp", "tp"), None),
        P(("sp", "tp"), None),
        P("sp", None, "tp"),
        P("sp", None, "tp"),
        P("sp", None, "tp"),
    )
    return jax.shard_map(
        local, mesh=mesh, in_specs=placed, out_specs=P(("sp", "tp"), None), check_vma=False
    )
```

profile of v0, /device:TPU:1, one launch (start us, length us, event | category | flops | bytes accessed | tf_op | source)
XLA Modules:
  0.0 404.1 jit_solution(18025123581853373027)
XLA Ops:
  8.1 3.3 collective-permute-start
  13.9 2.7 multiply_reduce_fusion.1
  20.7 2.7 multiply_reduce_fusion
  23.4 6.7 %collective-permute-done.1 = bf16[1024,256]{1,0:T(8,128)(2,1)S(1)} collective-permute-done((bf16[1024,256]{1,0:T(8,128)(2,1)S(1)}, bf16[1024,256]{1,0:T(8,128)(2,1)S(1)}, u32[]{:S(2)}, u32[]{:S(2)}) %collective-permute-start.1) | collective-permute-done | bytes 524320 | tf_op jit(solution)/shard_map/ppermute | solution.py:14
  31.6 9.7 %collective-permute-done.3 = bf16[1024,256]{0,1:T(8,128)(2,1)S(1)} collective-permute-done((bf16[1024,256]{0,1:T(8,128)(2,1)}, bf16[1024,256]{0,1:T(8,128)(2,1)S(1)}, u32[]{:S(2)}, u32[]{:S(2)}) %collective-permute-start.3) | collective-permute-done | bytes 524320 | tf_op jit(solution)/shard_map/ppermute | solution.py:14
  55.9 10.5 %collective-permute-done.5 = bf16[2048,256]{0,1:T(8,128)(2,1)S(1)} collective-permute-done((bf16[2048,256]{0,1:T(8,128)(2,1)S(1)}, bf16[2048,256]{0,1:T(8,128)(2,1)S(1)}, u32[]{:S(2)}, u32[]{:S(2)}) %collective-permute-start.5) | collective-permute-done | bytes 1048608 | tf_op jit(solution)/shard_map/ppermute | solution.py:14
  69.0 2.5 copy.141
  71.6 17.3 %collective-permute-done.4 = bf16[2048,256]{1,0:T(8,128)(2,1)S(1)} collective-permute-done((bf16[2048,256]{1,0:T(8,128)(2,1)}, bf16[2048,256]{1,0:T(8,128)(2,1)S(1)}, u32[]{:S(2)}, u32[]{:S(2)}) %collective-permute-start.4) | collective-permute-done | bytes 1048608 | tf_op jit(solution)/shard_map/ppermute | solution.py:14
  91.7 4.6 %copy.140 = bf16[2,1024,2,2,64]{1,4,3,2,0:T(8,128)(2,1)S(1)} copy(bf16[2,1024,2,2,64]{4,3,2,1,0:T(2,128)(2,1)} %reshape.200) | data formatting | bytes 2097152 | tf_op jit(solution)/shard_map/while | solution.py:96
  96.4 3.2 pad_maximum_fusion.1
  102.8 10.4 %while.4 = (s32[]{:T(128)}, f32[2,2,512]{2,1,0:T(2,128)S(1)}, f32[2,2,512]{2,1,0:T(2,128)S(1)}, f32[2,2,512,128]{3,2,1,0:T(8,128)S(1)}, bf16[2,1024,2,2,64]{1,4,...) while((s32[]{:T(128)}, f32[2,2,512]{2,1,0:T(2,128)S(1)}, ...), condition=%wide.region_9.10_spmd, body=%wide.region_6.9_spmd.sunk | while | flops 822611968 | bytes 28704860 | solution.py:96
  105.5 2.4 fusion.149
  110.7 2.4 fusion.149
  113.2 31.8 %collective-permute-done.7 = bf16[4096,256]{0,1:T(8,128)(2,1)} collective-permute-done((bf16[4096,256]{0,1:T(8,128)(2,1)}, bf16[4096,256]{0,1:T(8,128)(2,1)}, u32[]{:S(2)}, u32[]{:S(2)}) %collective-permute-start.7) | collective-permute-done | bytes 2097184 | tf_op jit(solution)/shard_map/ppermute | solution.py:14
  145.0 4.5 %reshape.203 = bf16[4,1024,2,128]{1,0,3,2:T(4,128)(2,1)} reshape(bf16[4096,256]{0,1:T(8,128)(2,1)} %collective-permute-done.7) | data formatting | bytes 4194304 | tf_op jit(solution)/shard_map/reshape | solution.py:71
  149.5 3.4 copy.146
  153.0 37.0 %collective-permute-done.6 = bf16[4096,256]{1,0:T(8,128)(2,1)} collective-permute-done((bf16[4096,256]{1,0:T(8,128)(2,1)}, bf16[4096,256]{1,0:T(8,128)(2,1)}, u32[]{:S(2)}, u32[]{:S(2)}) %collective-permute-start.6) | collective-permute-done | bytes 2097184 | tf_op jit(solution)/shard_map/ppermute | solution.py:14
  189.9 8.3 %reshape.202 = bf16[4,1024,2,2,64]{4,3,2,1,0:T(2,128)(2,1)} reshape(bf16[4096,256]{1,0:T(8,128)(2,1)} %collective-permute-done.6) | data formatting | bytes 4194304 | tf_op jit(solution)/shard_map/reshape | solution.py:70
  198.2 10.6 %copy.145 = bf16[4,1024,2,2,64]{1,4,3,2,0:T(8,128)(2,1)} copy(bf16[4,1024,2,2,64]{4,3,2,1,0:T(2,128)(2,1)} %reshape.202) | data formatting | bytes 4194304 | tf_op jit(solution)/shard_map/while | solution.py:96
  208.9 25.2 %while.5 = (s32[]{:T(128)}, f32[2,2,512]{2,1,0:T(2,128)S(1)}, f32[2,2,512]{2,1,0:T(2,128)S(1)}, f32[2,2,512,128]{3,2,1,0:T(8,128)S(1)}, bf16[4,1024,2,2,64]{1,4,...) while((s32[]{:T(128)}, f32[2,2,512]{2,1,0:T(2,128)S(1)}, ...), condition=%wide.region_13.14_spmd, body=%wide.region_10.13_spmd.sunk | while | flops 822611968 | bytes 28705368 | solution.py:96
  212.7 2.4 fusion.154
  225.2 2.4 fusion.154
  236.2 3.4 all-to-all-start
  239.7 5.4 %all-to-all-done = bf16[4,128,256]{2,1,0:T(8,128)(2,1)S(1)} async-done(((bf16[4,128,256]{2,1,0:T(8,128)(2,1)}), bf16[4,128,256]{2,1,0:T(8,128)(2,1)S(1)}, u32[]{:S(2)}, u32[]{:S(2)}) %all-to-all-start) | async-done | bytes 262176 | tf_op jit(solution)/shard_map/all_to_all | solution.py:124
  245.3 3.0 multiply_reduce_fusion.3
  250.5 14.8 %all-to-all-start.1 = ((bf16[64,1,8,2048]{3,2,1,0:T(8,128)(2,1)}), bf16[64,1,8,2048]{3,2,1,0:T(8,128)(2,1)S(1)}, u32[]{:S(2)}, u32[]{:S(2)}) async-start(bf16[64,1,8,2048]{3,2,1,0:T(8,128)(2,1)} %fusion.56), calls=%async_computation.1 | async-start | bytes 4194304 | tf_op jit(solution)/shard_map/all_to_all | solution.py:154
  265.3 49.7 %all-to-all-done.1 = bf16[64,1,8,2048]{3,2,1,0:T(8,128)(2,1)S(1)} async-done(((bf16[64,1,8,2048]{3,2,1,0:T(8,128)(2,1)}), bf16[64,1,8,2048]{3,2,1,0:T(8,128)(2,1)S(1)}, u32[]{:S(2)}, u32[]{:S(2)}) %all-to-all-start.1) | async-done | bytes 2097184 | tf_op jit(solution)/shard_map/all_to_all | solution.py:154
  315.0 5.9 %fusion.43 = f32[64,8,1024]{2,1,0:T(8,128)} fusion(bf16[1,2048,1024]{2,1,0:T(8,128)(2,1)} %all-gather.6.cloned.1.call-done, bf16[64,1,8,2048]{3,2,1,0:T(8,128)(2,1)S(1)} %all-to-all-done.1), kind=kOutput, calls=%fused_computation.47 | convolution fusion | flops 2147483648 | bytes 8388608 | tf_op jit(solution)/shard_map/secd,edf->secf/dot_general | solution.py:37
  320.9 10.0 %fusion.57 = bf16[64,1,8,2048]{3,2,1,0:T(8,128)(2,1)} fusion(bf16[1,2048,1024]{2,1,0:T(8,128)(2,1)} %all-gather.8.cloned.1.call-done, f32[64,8,1024]{2,1,0:T(8,128)} %fusion.43, bf16[1,2048,1024]{2,1,0:T(8,128)(2,1)} %all-gather.4.cloned.1.call-done, bf16[64,1,8,2048]{3,2,1,0:T(8,128)(2,1)S(1)} %all-to-all-done.1), kind=kOutput, calls=%fused_computation.64 | convolution fusion | flops 4299161600 | bytes 14680064 | tf_op jit(solution)/shard_map/secf,edf->secd/dot_general | solution.py:156
  330.9 7.5 %all-to-all-start.2 = ((bf16[64,1,8,2048]{3,2,1,0:T(8,128)(2,1)}), bf16[64,1,8,2048]{3,2,1,0:T(8,128)(2,1)S(1)}, u32[]{:S(2)}, u32[]{:S(2)}) async-start(bf16[64,1,8,2048]{3,2,1,0:T(8,128)(2,1)} %fusion.57), calls=%async_computation.2 | async-start | bytes 4194304 | tf_op jit(solution)/shard_map/all_to_all | solution.py:42
  338.9 49.0 %all-to-all-done.2 = bf16[64,1,8,2048]{3,2,1,0:T(8,128)(2,1)S(1)} async-done(((bf16[64,1,8,2048]{3,2,1,0:T(8,128)(2,1)}), bf16[64,1,8,2048]{3,2,1,0:T(8,128)(2,1)S(1)}, u32[]{:S(2)}, u32[]{:S(2)}) %all-to-all-start.2) | async-done | bytes 2097184 | tf_op jit(solution)/shard_map/all_to_all | solution.py:42
  392.0 4.1 %multiply_reduce_fusion.2 = f32[128,2048]{1,0:T(8,128)S(1)} fusion(bf16[128,2,2048]{2,1,0:T(2,128)(2,1)S(1)} %gather.7, pred[128,2]{1,0:T(8,128)(4,1)S(1)} %copy.153, f32[128,2]{1,0:T(8,128)S(1)} %copy.150), kind=kLoop, calls=%fused_computation.83 | loop fusion | flops 1835008 | bytes 2098432 | tf_op jit(solution)/shard_map/reduce_sum | solution.py:164
  (145 shorter events, 67.8 us)
Async XLA Ops:
  6.5 7.2 %copy-start.18 = (bf16[512,256]{1,0:T(8,128)(2,1)S(1)}, bf16[512,256]{1,0:T(8,128)(2,1)}, u32[]{:S(2)}) copy-start(bf16[512,256]{1,0:T(8,128)(2,1)} %param.17) | copy-start | bytes 786436
  6.5 258.8 %all-gather.6.cloned.1.call-start = ((), (), s32[]{:S(2)}) async-start(), calls=%async_computation.4 | async-start | bytes 5242880 | tf_op jit(solution)/shard_map/all_gather | solution.py:150
  7.3 9.3 %copy-start.19 = (s32[128,2]{0,1:T(2,128)S(1)}, s32[128,2]{0,1:T(2,128)}, u32[]{:S(2)}) copy-start(s32[128,2]{0,1:T(2,128)} %param.25) | copy-start | bytes 3076
  7.3 9.6 %copy-start.8 = (bf16[512,256]{1,0:T(8,128)(2,1)S(1)}, bf16[512,256]{1,0:T(8,128)(2,1)}, u32[]{:S(2)}) copy-start(bf16[512,256]{1,0:T(8,128)(2,1)} %param.18) | copy-start | bytes 786436
  7.3 313.6 %all-gather.4.cloned.1.call-start = ((), (), s32[]{:S(2)}) async-start(), calls=%async_computation.3 | async-start | bytes 5242880 | tf_op jit(solution)/shard_map/all_gather | solution.py:149
  8.0 9.1 %copy-start.15 = (bf16[512,256]{1,0:T(8,128)(2,1)S(1)}, bf16[512,256]{1,0:T(8,128)(2,1)}, u32[]{:S(2)}) copy-start(bf16[512,256]{1,0:T(8,128)(2,1)} %param.19) | copy-start | bytes 786436
  8.0 312.8 %all-gather.8.cloned.1.call-start = ((), (), s32[]{:S(2)}) async-start(), calls=%async_computation.5 | async-start | bytes 5242880 | tf_op jit(solution)/shard_map/all_gather | solution.py:151
  8.1 8.7 %collective-permute-start = (bf16[512,256]{1,0:T(8,128)(2,1)}, bf16[512,256]{1,0:T(8,128)(2,1)S(1)}, u32[]{:S(2)}, u32[]{:S(2)}) collective-permute-start(bf16[512,256]{1,0:T(8,128)(2,1)} %param.18), channel_id=1, source_target_pairs={{0,4},{4,0},{8,12},{12,8},{16,20},{20,16},{24,28},{28,24},{32,36},... | collective-permute-start | bytes 786440 | tf_op jit(solution)/shard_map/ppermute | solution.py:14
  12.5 28.8 %copy-start.12 = (bf16[512,256]{0,1:T(8,128)(2,1)}, bf16[512,256]{0,1:T(8,128)(2,1)S(1)}, u32[]{:S(2)}) copy-start(bf16[512,256]{0,1:T(8,128)(2,1)S(1)} %copy.131) | copy-start | bytes 786436
  12.5 5.7 %collective-permute-start.2 = (bf16[512,256]{0,1:T(8,128)(2,1)S(1)}, bf16[512,256]{0,1:T(8,128)(2,1)S(1)}, u32[]{:S(2)}, u32[]{:S(2)}) collective-permute-start(bf16[512,256]{0,1:T(8,128)(2,1)S(1)} %copy.131), channel_id=1, source_target_pairs={{0,4},{4,0},{8,12},{12,8},{16,20},{20,16},{24,28},{28,24},{32,36},... | collective-permute-start | bytes 786440 | tf_op jit(solution)/shard_map/ppermute | solution.py:14
  16.8 25.9 %copy-start.10 = (bf16[512,256]{1,0:T(8,128)(2,1)}, bf16[512,256]{1,0:T(8,128)(2,1)S(1)}, u32[]{:S(2)}) copy-start(bf16[512,256]{1,0:T(8,128)(2,1)S(1)} %collective-permute-done) | copy-start | bytes 786436
  16.9 13.2 %collective-permute-start.1 = (bf16[1024,256]{1,0:T(8,128)(2,1)S(1)}, bf16[1024,256]{1,0:T(8,128)(2,1)S(1)}, u32[]{:S(2)}, u32[]{:S(2)}) collective-permute-start(bf16[1024,256]{1,0:T(8,128)(2,1)S(1)} %pad_maximum_fusion.4), channel_id=1, source_target_pairs={{0,8},{4,12},{8,0},{12,4},{16,24},{20,28},{24,16},{28,20},{32,40},... | collective-permute-start | bytes 1572872 | tf_op jit(solution)/shard_map/ppermute | solution.py:14
  18.2 23.1 %copy-start.13 = (bf16[512,256]{0,1:T(8,128)(2,1)}, bf16[512,256]{0,1:T(8,128)(2,1)S(1)}, u32[]{:S(2)}) copy-start(bf16[512,256]{0,1:T(8,128)(2,1)S(1)} %collective-permute-done.2) | copy-start | bytes 786436
  19.1 22.2 %collective-permute-start.3 = (bf16[1024,256]{0,1:T(8,128)(2,1)}, bf16[1024,256]{0,1:T(8,128)(2,1)S(1)}, u32[]{:S(2)}, u32[]{:S(2)}) collective-permute-start(bf16[1024,256]{0,1:T(8,128)(2,1)} %pad_maximum_fusion.5), channel_id=1, source_target_pairs={{0,8},{4,12},{8,0},{12,4},{16,24},{20,28},{24,16},{28,20},{32,40},... | collective-permute-start | bytes 1572872 | tf_op jit(solution)/shard_map/ppermute | solution.py:14
  30.1 12.6 %copy-start.3 = (bf16[1024,256]{1,0:T(8,128)(2,1)}, bf16[1024,256]{1,0:T(8,128)(2,1)S(1)}, u32[]{:S(2)}) copy-start(bf16[1024,256]{1,0:T(8,128)(2,1)S(1)} %collective-permute-done.1) | copy-start | bytes 1572868
  41.3 10.9 %copy-start.2 = (bf16[1024,256]{0,1:T(8,128)(2,1)}, bf16[1024,256]{0,1:T(8,128)(2,1)S(1)}, u32[]{:S(2)}) copy-start(bf16[1024,256]{0,1:T(8,128)(2,1)S(1)} %collective-permute-done.3) | copy-start | bytes 1572868
  41.4 25.1 %collective-permute-start.5 = (bf16[2048,256]{0,1:T(8,128)(2,1)S(1)}, bf16[2048,256]{0,1:T(8,128)(2,1)S(1)}, u32[]{:S(2)}, u32[]{:S(2)}) collective-permute-start(bf16[2048,256]{0,1:T(8,128)(2,1)S(1)} %pad_maximum_fusion.3), channel_id=1, source_target_pairs={{0,16},{4,20},{8,24},{12,28},{16,0},{20,4},{24,8},{28,12},{32,48},... | collective-permute-start | bytes 3145736 | tf_op jit(solution)/shard_map/ppermute | solution.py:14
  43.8 45.2 %collective-permute-start.4 = (bf16[2048,256]{1,0:T(8,128)(2,1)}, bf16[2048,256]{1,0:T(8,128)(2,1)S(1)}, u32[]{:S(2)}, u32[]{:S(2)}) collective-permute-start(bf16[2048,256]{1,0:T(8,128)(2,1)} %pad_maximum_fusion.2), channel_id=1, source_target_pairs={{0,16},{4,20},{8,24},{12,28},{16,0},{20,4},{24,8},{28,12},{32,48},... | collective-permute-start | bytes 3145736 | tf_op jit(solution)/shard_map/ppermute | solution.py:14
  45.7 3.5 copy-start.1
  96.4 3.3 copy-start.4
  96.4 3.3 copy-start.6
  96.4 3.3 copy-start.9
  99.6 45.4 %collective-permute-start.7 = (bf16[4096,256]{0,1:T(8,128)(2,1)}, bf16[4096,256]{0,1:T(8,128)(2,1)}, u32[]{:S(2)}, u32[]{:S(2)}) collective-permute-start(bf16[4096,256]{0,1:T(8,128)(2,1)} %pad_maximum_fusion.1), channel_id=1, source_target_pairs={{0,32},{4,36},{8,40},{12,44},{16,48},{20,52},{24,56},{28,60},{32,0... | collective-permute-start | bytes 6291464 | tf_op jit(solution)/shard_map/ppermute | solution.py:14
  101.1 88.8 %collective-permute-start.6 = (bf16[4096,256]{1,0:T(8,128)(2,1)}, bf16[4096,256]{1,0:T(8,128)(2,1)}, u32[]{:S(2)}, u32[]{:S(2)}) collective-permute-start(bf16[4096,256]{1,0:T(8,128)(2,1)} %pad_maximum_fusion), channel_id=1, source_target_pairs={{0,32},{4,36},{8,40},{12,44},{16,48},{20,52},{24,56},{28,60},{32,0... | collective-permute-start | bytes 6291464 | tf_op jit(solution)/shard_map/ppermute | solution.py:14
  208.9 25.6 %copy-start.21 = (f32[2]{0:T(128)S(1)}, f32[2]{0:T(128)}, u32[]{:S(2)}) copy-start(f32[2]{0:T(128)} %param.20) | copy-start | bytes 28
  208.9 25.9 %copy-start.23 = (f32[128]{0:T(128)S(1)}, f32[128]{0:T(128)}, u32[]{:S(2)}) copy-start(f32[128]{0:T(128)} %param.21) | copy-start | bytes 1540
  234.2 11.2 %copy-start.17 = (bf16[128,2048]{1,0:T(8,128)(2,1)S(1)}, bf16[128,2048]{1,0:T(8,128)(2,1)}, u32[]{:S(2)}) copy-start(bf16[128,2048]{1,0:T(8,128)(2,1)} %param.23) | copy-start | bytes 1572868
  235.1 13.3 %copy-start.20 = (f32[2048]{0:T(1024)S(1)}, f32[2048]{0:T(1024)}, u32[]{:S(2)}) copy-start(f32[2048]{0:T(1024)} %param.24) | copy-start | bytes 24580
  236.2 8.9 %all-to-all-start = ((bf16[4,128,256]{2,1,0:T(8,128)(2,1)}), bf16[4,128,256]{2,1,0:T(8,128)(2,1)S(1)}, u32[]{:S(2)}, u32[]{:S(2)}) async-start(bf16[4,128,256]{2,1,0:T(8,128)(2,1)} %convert_element_type.86), calls=%async_computation | async-start | bytes 524288 | tf_op jit(solution)/shard_map/all_to_all | solution.py:124
  250.5 64.5 %all-to-all-start.1 = ((bf16[64,1,8,2048]{3,2,1,0:T(8,128)(2,1)}), bf16[64,1,8,2048]{3,2,1,0:T(8,128)(2,1)S(1)}, u32[]{:S(2)}, u32[]{:S(2)}) async-start(bf16[64,1,8,2048]{3,2,1,0:T(8,128)(2,1)} %fusion.56), calls=%async_computation.1 | async-start | bytes 4194304 | tf_op jit(solution)/shard_map/all_to_all | solution.py:154
  330.9 7.9 %copy-start.22 = (f32[128,2]{0,1:T(2,128)S(1)}, f32[128,2]{0,1:T(2,128)}, u32[]{:S(2)}) copy-start(f32[128,2]{0,1:T(2,128)} %param.26) | copy-start | bytes 3076
  330.9 57.1 %all-to-all-start.2 = ((bf16[64,1,8,2048]{3,2,1,0:T(8,128)(2,1)}), bf16[64,1,8,2048]{3,2,1,0:T(8,128)(2,1)S(1)}, u32[]{:S(2)}, u32[]{:S(2)}) async-start(bf16[64,1,8,2048]{3,2,1,0:T(8,128)(2,1)} %fusion.57), calls=%async_computation.2 | async-start | bytes 4194304 | tf_op jit(solution)/shard_map/all_to_all | solution.py:42
  (6 other events, 11.1 us)
Sparse Core Ops, SparseCore 0:
  9.1 56.3 all-gather.5
  67.3 54.8 all-gather.3
  124.0 54.8 all-gather.7
where the time goes:
time: 411 us; the launch traced here: 404 us
  waiting for transfers between devices  219 us (53%)
  matrix products  59.6 us (15%)
  local copies, waits for them, and re-layouts  51.5 us (13%)
  starting transfers between devices  35.6 us (9%)
  other arithmetic  24.2 us (6%)
  between operations  14.1 us (3%)
    ppermute x8, waiting for transfers between devices, swapped(): return lax.ppermute(value, axis, pairs)  113 us
    all_to_all x1, waiting for transfers between devices, local(): lax.all_to_all(outgoing, 'sp', split_axis=0, concat_axis=0, tiled=True)  49.7 us
    all_to_all x1, waiting for transfers between devices, send_back(): lax.all_to_all(results, 'sp', split_axis=0, concat_axis=0, tiled=True)  49 us
    while x4, local copies, waits for them, and re-layouts, absorb(): lax.scan(one_block, running, (key_blocks, value_blocks))  21.3 us
    dot_general x9, matrix products, one_block(): jnp.einsum('hmqk,khv->hmqv', weights.astype(jnp.bfloat16), value_block, p...  19.8 us
    dot_general x9, matrix products, one_block(): jnp.einsum('qhmd,khmd->hmqk', query_view, key_block, preferred_element_ty...  18.8 us
    all_to_all x1, starting transfers between devices, local(): lax.all_to_all(outgoing, 'sp', split_axis=0, concat_axis=0, tiled=True)  14.8 us
    reduce_sum x8, other arithmetic, one_block(): new_sum = running_sum * shrink + jnp.sum(weights, axis=-1)  11.1 us
  transfers between devices with their start and end apart: 14, of which 9 were waited for; matrix products, arithmetic and copies ran while one was open for 28% of the time, Pallas kernels for 0%

commit v1 on v0

v1 whole, which is shorter than its diff:
```python
import functools
import jax
import jax.numpy as jnp
from jax import lax
from jax.experimental import pallas as pl
from jax.experimental.pallas import tpu as pltpu
from jax.sharding import PartitionSpec as P

EPSILON = 1e-06
OUT_SCALE = 0.8
FLOOR_SCORE = -1e30
LOG2E = 1.4426950408889634
MESH = pl.DeviceIdType.MESH


def attend_kernel(lam_ref, gain_ref, q_ref, k_ref, v_ref, o_ref,
                  kbuf, vbuf, qbuf, qz, sbuf, ebuf, acc, mrun, att,
                  ssem, rsem, qsem, osend, orecv):
    s = lax.axis_index("sp")
    x = lax.axis_index("tp")
    rows = q_ref.shape[2]
    zb = (s // 8) % 2
    y = (s // 2) % 4
    c = s % 2
    mine = s % 16
    base = s - mine
    y1 = y + 1 - 2 * (y % 2)
    y3 = 3 - y
    y2 = (y + 2) % 4

    def slot_of(zz, yy, cc):
        return zz * 8 + yy * 2 + cc

    zpeer = base + slot_of(1 - zb, y, c)
    y1dev = base + slot_of(zb, y1, c)
    y3dev = base + slot_of(zb, y3, c)
    twin = base + slot_of(zb, y, 1 - c)

    barrier = pltpu.get_barrier_semaphore()
    peers = [(zpeer, x), (y1dev, x), (y3dev, x), (twin, x)]
    for j in range(1, 4):
        peers.append((s, (x + j) % 4))
        peers.append((zpeer, (x + j) % 4))
    for ps, px in peers:
        pl.semaphore_signal(barrier, inc=1, device_id={"sp": ps, "tp": px}, device_id_type=MESH)
    pl.semaphore_wait(barrier, len(peers))

    def kslot(slot):
        return kbuf.at[slot // 2, pl.ds(pl.multiple_of((slot % 2) * rows, rows), rows)]

    def vslot(slot):
        return vbuf.at[slot, pl.ds(0, 128)]

    def pair_copy(ksrc, vsrc, slot, dest, idx):
        return (
            pltpu.make_async_remote_copy(ksrc, kslot(slot), ssem.at[idx, 0], rsem.at[slot, 0],
                                         device_id={"sp": dest, "tp": x}, device_id_type=MESH),
            pltpu.make_async_remote_copy(vsrc, vslot(slot), ssem.at[idx, 1], rsem.at[slot, 1],
                                         device_id={"sp": dest, "tp": x}, device_id_type=MESH),
        )

    def start(pair):
        pair[0].start()
        pair[1].start()

    def forward(slot, dest, idx):
        start(pair_copy(kslot(slot), vslot(slot), slot, dest, idx))

    def wait_slot(slot):
        a, b = pair_copy(kslot(slot), vslot(slot), slot, twin, 0)
        a.wait_recv()
        b.wait_recv()

    qcopy = pltpu.make_async_remote_copy(q_ref.at[1 - zb], qbuf, qsem.at[0], qsem.at[1],
                                         device_id={"sp": zpeer, "tp": x}, device_id_type=MESH)
    qcopy.start()
    own_k, own_v = k_ref.at[zb], v_ref.at[zb]
    start(pair_copy(own_k, own_v, mine, twin, 3))
    start(pair_copy(k_ref.at[1 - zb], v_ref.at[1 - zb], mine, zpeer, 0))
    start(pair_copy(own_k, own_v, mine, y1dev, 1))
    start(pair_copy(own_k, own_v, mine, y3dev, 2))

    kbuf[mine // 2, pl.ds(pl.multiple_of(c * rows, rows), rows), :] = k_ref[zb]
    vbuf[mine, pl.ds(0, 128), :] = v_ref[zb]
    for slot in range(16):
        vbuf[slot, pl.ds(128, 16), :] = jnp.ones((16, rows), jnp.bfloat16)
    zeros = jnp.zeros((64, rows), jnp.bfloat16)

    def put_queries(value, column):
        qz[pl.ds(0, 64), pl.ds(column, rows)] = value[:64]
        qz[pl.ds(64, 64), pl.ds(column, rows)] = zeros
        qz[pl.ds(0, 64), pl.ds(2 * rows + column, rows)] = zeros
        qz[pl.ds(64, 64), pl.ds(2 * rows + column, rows)] = value[64:]

    put_queries(q_ref[zb], 0)
    mrun[...] = jnp.full(mrun.shape, FLOOR_SCORE, jnp.float32)
    acc[...] = jnp.zeros(acc.shape, jnp.float32)
    qcopy.wait_recv()
    put_queries(qbuf[...], rows)

    scale = LOG2E * 64 ** (-0.5)
    keys_here = 2 * rows
    tiles = 2 * 2 * rows // 256
    per_map = tiles // 2

    def scores(p, t):
        column = t * 256
        top = None
        for part in range(2):
            value = jnp.dot(kbuf[p, pl.ds(part * rows, rows), :], qz[:, pl.ds(column, 256)],
                            preferred_element_type=jnp.float32)
            sbuf[t % 2, pl.ds(part * rows, rows), :] = value
            peak = jnp.max(value.reshape(rows // 8, 8, 256), axis=0)
            top = peak if top is None else jnp.maximum(top, peak)
        return jnp.max(top, axis=0, keepdims=True) * scale

    def weigh(t, peak):
        old = mrun[t]
        new = jnp.maximum(old, peak)
        mrun[t] = new
        for part in range(4):
            here = pl.ds(part * keys_here // 4, keys_here // 4)
            ebuf[t % 2, here, :] = jnp.exp2(sbuf[t % 2, here, :] * scale - new).astype(jnp.bfloat16)
        return jnp.exp2(old - new)

    def gather_values(p, t, shrink):
        product = jnp.dot(vbuf[2 * p], ebuf[t % 2, pl.ds(0, rows), :], preferred_element_type=jnp.float32)
        product += jnp.dot(vbuf[2 * p + 1], ebuf[t % 2, pl.ds(rows, rows), :], preferred_element_type=jnp.float32)
        acc[t] = acc[t] * shrink + product

    def compute(p):
        peak = scores(p, 0)
        for t in range(tiles):
            following = scores(p, t + 1) if t + 1 < tiles else None
            shrink = weigh(t, peak)
            gather_values(p, t, shrink)
            peak = following

    order = [(0, y), (1, y), (0, y1), (1, y1), (0, y3), (1, y3), (0, y2), (1, y2)]

    def comm(i):
        flip, yy = order[i]
        zz = zb + flip - 2 * zb * flip
        slot = slot_of(zz, yy, c)
        wait_slot(slot)
        if i == 1:
            forward(slot, y1dev, 4)
            forward(slot, y3dev, 5)
        if i == 2:
            forward(slot, y3dev, 8)
        if i == 5:
            forward(slot, y1dev, 12)
        forward(slot, twin, {1: 6, 2: 7, 3: 9, 4: 10, 5: 11, 6: 13, 7: 14}[i])

    def step(i, carry):
        @pl.when(i == 1)
        def _():
            comm(1)
            comm(2)
        for k in range(3, 8):
            @pl.when(i == k - 1)
            def _(k=k):
                comm(k)
        j = i // 2
        gray = j + (j // 2) - 2 * (j // 2) * (j % 2)
        lo, hi = gray % 2, gray // 2
        yhi, ylo = y // 2, y % 2
        yy = 2 * (yhi + hi - 2 * yhi * hi) + (ylo + lo - 2 * ylo * lo)
        flip = i % 2
        zz = zb + flip - 2 * zb * flip
        wait_slot(slot_of(zz, yy, 1 - c))
        compute(zz * 4 + yy)
        return carry

    lax.fori_loop(0, 8, step, 0)

    lam = lam_ref[0, 0]
    gain = gain_ref[...]
    head = 2 * x + zb
    for qt in (2, 3, 0, 1):
        first, second = acc[qt], acc[per_map + qt]
        combined = first[:128] / first[128:129] - lam * (second[:128] / second[128:129])
        mean_square = jnp.mean(combined * combined, axis=0, keepdims=True)
        value = (combined * lax.rsqrt(mean_square + EPSILON) * gain).astype(jnp.bfloat16)
        att[2 * qt] = value[:, :128]
        att[2 * qt + 1] = value[:, 128:]

    sends = []
    for j in range(4):
        xx = (x + j) % 4
        sends.append(pltpu.make_async_remote_copy(
            att.at[4 + xx], o_ref.at[head], osend.at[j], orecv.at[head],
            device_id={"sp": zpeer, "tp": xx}, device_id_type=MESH))
        sends[-1].start()
    for j in range(1, 4):
        xx = (x + j) % 4
        sends.append(pltpu.make_async_remote_copy(
            att.at[xx], o_ref.at[head], osend.at[3 + j], orecv.at[head],
            device_id={"sp": s, "tp": xx}, device_id_type=MESH))
        sends[-1].start()
    o_ref[head] = att[x]
    for j in range(4):
        xx = (x + j) % 4
        for far in range(2):
            if j == 0 and far == 0:
                continue
            hh = 2 * xx + (1 - zb if far else zb)
            pltpu.make_async_remote_copy(
                att.at[0], o_ref.at[hh], osend.at[0], orecv.at[hh],
                device_id={"sp": zpeer, "tp": x}, device_id_type=MESH).wait_recv()
    for copy in sends:
        copy.wait_send()
    qcopy.wait_send()
    for idx in range(15):
        a, b = pair_copy(own_k, own_v, mine, twin, idx)
        a.wait_send()
        b.wait_send()


def attend(queries, keys, values, lambdas, head_gain):
    rows = queries.shape[0]
    zb = (lax.axis_index("sp") // 8) % 2
    q = jnp.transpose(queries.reshape(rows, 2, 128), (1, 2, 0))
    k = jnp.transpose(keys.reshape(rows, 2, 128), (1, 0, 2))
    v = jnp.transpose(values.reshape(rows, 2, 128), (1, 2, 0))
    lam = lax.dynamic_slice(lambdas, (zb,), (1,)).reshape(1, 1)
    gain = (head_gain * OUT_SCALE).reshape(128, 1)
    bf, f32 = jnp.bfloat16, jnp.float32
    tiles = 4 * rows // 256
    vm = pl.BlockSpec(memory_space=pltpu.VMEM)
    return pl.pallas_call(
        attend_kernel,
        out_shape=jax.ShapeDtypeStruct((8, 128, 128), bf),
        in_specs=[pl.BlockSpec(memory_space=pltpu.SMEM), vm, vm, vm, vm],
        out_specs=vm,
        scratch_shapes=[
            pltpu.VMEM((8, 2 * rows, 128), bf),
            pltpu.VMEM((16, 144, rows), bf),
            pltpu.VMEM((128, rows), bf),
            pltpu.VMEM((128, 4 * rows), bf),
            pltpu.VMEM((2, 2 * rows, 256), f32),
            pltpu.VMEM((2, 2 * rows, 256), bf),
            pltpu.VMEM((tiles, 144, 256), f32),
            pltpu.VMEM((tiles, 1, 256), f32),
            pltpu.VMEM((8, 128, 128), bf),
            pltpu.SemaphoreType.DMA((15, 2)),
            pltpu.SemaphoreType.DMA((16, 2)),
            pltpu.SemaphoreType.DMA((2,)),
            pltpu.SemaphoreType.DMA((7,)),
            pltpu.SemaphoreType.DMA((8,)),
        ],
        compiler_params=pltpu.CompilerParams(collective_id=1, has_side_effects=True,
                                             vmem_limit_bytes=40 * 1024 * 1024),
        name="attend",
    )(lam, gain, q, k, v)


def slot_numbers(flat_ids):
    count_ids = flat_ids.shape[0]
    positions = lax.broadcasted_iota(jnp.int32, (count_ids, count_ids), 0)
    earlier = lax.broadcasted_iota(jnp.int32, (count_ids, count_ids), 1) < positions
    matches = (flat_ids[:, None] == flat_ids[None, :]) & earlier
    return jnp.sum(matches.astype(jnp.int32), axis=1)


def expert_hidden(arrived, gate_weight, up_weight):
    gate_proj = jnp.einsum("secd,edf->secf", arrived, gate_weight, preferred_element_type=jnp.float32)
    up_proj = jnp.einsum("secd,edf->secf", arrived, up_weight, preferred_element_type=jnp.float32)
    return (jax.nn.silu(gate_proj) * up_proj).astype(jnp.bfloat16)


def send_back(results):
    return lax.all_to_all(results, "sp", split_axis=0, concat_axis=0, tiled=True)


def local(queries, keys, values, lambdas, head_gain, w_out, residual_in, norm_gain,
          route_ids, route_weight, w_gate, w_up, w_down):
    attended = attend(queries, keys, values, lambdas, head_gain).reshape(8 * 128, 128)
    dev_rows = residual_in.shape[0]
    mixed_sum = lax.dot_general(attended, w_out, (((0,), (0,)), ((), ())), preferred_element_type=jnp.float32)
    mixed_out = mixed_sum.astype(jnp.bfloat16)
    carried = (residual_in.astype(jnp.float32) + mixed_out.astype(jnp.float32)).astype(jnp.bfloat16)
    carried_wide = carried.astype(jnp.float32)
    normed = (
        carried_wide
        * lax.rsqrt(jnp.mean(carried_wide * carried_wide, axis=-1, keepdims=True) + EPSILON)
        * norm_gain
    ).astype(jnp.bfloat16)
    model_width = normed.shape[1]
    experts_here = w_gate.shape[0]
    expert_count = experts_here * lax.axis_size("sp")
    capacity = max(2, 4 * dev_rows // expert_count)
    flat_ids = route_ids.reshape(-1)
    targets = flat_ids * capacity + slot_numbers(flat_ids)
    slot_ids = lax.broadcasted_iota(jnp.int32, (expert_count * capacity, dev_rows, 2), 0)
    placement_matrix = jnp.sum(
        (targets.reshape(1, dev_rows, 2) == slot_ids).astype(jnp.int32), axis=2
    ).astype(jnp.bfloat16)
    outgoing = jnp.dot(placement_matrix, normed, preferred_element_type=jnp.float32).astype(jnp.bfloat16)
    outgoing = outgoing.reshape(lax.axis_size("sp"), experts_here, capacity, model_width)
    full_gate, full_up, full_down = (
        lax.all_gather(w_gate, "tp", axis=2, tiled=True),
        lax.all_gather(w_up, "tp", axis=2, tiled=True),
        lax.all_gather(w_down, "tp", axis=2, tiled=True),
    )
    hidden_units = expert_hidden(
        lax.all_to_all(outgoing, "sp", split_axis=0, concat_axis=0, tiled=True), full_gate, full_up
    )
    summed = jnp.einsum("secf,edf->secd", hidden_units, full_down, preferred_element_type=jnp.float32)
    returned = send_back(summed.astype(jnp.bfloat16))
    flat_back = returned.reshape(expert_count * capacity, model_width)
    picked = jnp.take(flat_back, targets, axis=0).astype(jnp.float32).reshape(dev_rows, 2, model_width)
    layer_out = carried_wide + jnp.sum(route_weight[..., None] * picked, axis=1)
    return layer_out.astype(jnp.bfloat16)


def solution(mesh):
    placed = (
        P("sp", "tp"), P("sp", "tp"), P("sp", "tp"), P("tp"), P(), P(),
        P(("sp", "tp"), None), P(), P(("sp", "tp"), None), P(("sp", "tp"), None),
        P("sp", None, "tp"), P("sp", None, "tp"), P("sp", None, "tp"),
    )
    return jax.shard_map(local, mesh=mesh, in_specs=placed, out_specs=P(("sp", "tp"), None), check_vma=False)
```

time: 411 us -> 269 us (0.65); the launches traced: 404 us -> 268 us
  waiting for transfers between devices: 219 us -> 101 us
  blocking collectives: 0 us -> 60.8 us
  Pallas kernels: 0 us -> 49.3 us
  local copies, waits for them, and re-layouts: 51.5 us -> 6.38 us
  matrix products: 59.6 us -> 19.6 us
  starting transfers between devices: 35.6 us -> 12.3 us
  other arithmetic: 24.2 us -> 5.3 us
    ppermute x8 -> x0, waiting for transfers between devices: 113 us -> none  [swapped(): return lax.ppermute(value, axis, pairs)]
    all_to_all x0 -> x1, blocking collectives: none -> 60.8 us  [local(): lax.all_to_all(outgoing, 'sp', split_axis=0, concat_axis=0, tiled=True)]
    all_to_all x2 -> x0, waiting for transfers between devices: 55.1 us -> none  [the longest x1 49.7 us: local(): lax.all_to_all(outgoing, 'sp', split_axis=0, concat_axis=0, tiled=True)]
    all_gather x1, waiting for transfers between devices: 0.01 us -> 50 us  [local(): lax.all_gather(w_down, 'tp', axis=2, tiled=True)]
    pallas_call x0 -> x1, Pallas kernels: none -> 49.3 us  [attend(): pl.pallas_call(attend_kernel, out_shape=jax.ShapeDtypeStruct((8, 128, 128...]
    dot_general x19 -> x1, matrix products: 41.6 us -> 3.01 us  [local(): lax.dot_general(attended, w_out, (((0,), (0,)), ((), ())), preferred_elem...]
    while x10 -> x0, local copies, waits for them, and re-layouts: 21.3 us -> none  [the longest x4 21.3 us: absorb(): lax.scan(one_block, running, (key_blocks, value_blocks))]
    all_to_all x2 -> x0, starting transfers between devices: 18.2 us -> none  [the longest x1 14.8 us: local(): lax.all_to_all(outgoing, 'sp', split_axis=0, concat_axis=0, tiled=True)]
  transfers between devices with their start and end apart: 14 -> 4, of which waited for: 9 -> 2; matrix products, arithmetic and copies ran while one was open for 28% -> 5% of each run, Pallas kernels for 0% -> 18%
where the time goes in v1:
time: 269 us; the launch traced here: 268 us
  waiting for transfers between devices  101 us (38%)
  blocking collectives  60.8 us (23%)
  Pallas kernels  49.3 us (18%)
  matrix products  19.6 us (7%)
  between operations  13.4 us (5%)
  starting transfers between devices  12.3 us (5%)
  local copies, waits for them, and re-layouts  6.38 us (2%)
  other arithmetic  5.3 us (2%)
    all_to_all x1, blocking collectives, local(): lax.all_to_all(outgoing, 'sp', split_axis=0, concat_axis=0, tiled=True)  60.8 us
    all_gather x1, waiting for transfers between devices, local(): lax.all_gather(w_down, 'tp', axis=2, tiled=True)  50 us
    pallas_call x1, Pallas kernels, attend(): pl.pallas_call(attend_kernel, out_shape=jax.ShapeDtypeStruct((8, 128, 128...  49.3 us
    all_to_all x1, waiting for transfers between devices, send_back(): lax.all_to_all(results, 'sp', split_axis=0, concat_axis=0, tiled=True)  49.2 us
    all_to_all x1, starting transfers between devices, send_back(): lax.all_to_all(results, 'sp', split_axis=0, concat_axis=0, tiled=True)  12.2 us
    dot_general x1, matrix products, local(): jnp.einsum('secf,edf->secd', hidden_units, full_down, preferred_element_t...  9.98 us
    dot_general x1, matrix products, expert_hidden(): jnp.einsum('secd,edf->secf', arrived, up_weight, preferred_element_type=j...  5.84 us
  transfers between devices with their start and end apart: 4, of which 2 were waited for; matrix products, arithmetic and copies ran while one was open for 5% of the time, Pallas kernels for 18%

profile of v1, /device:TPU:1, one launch (start us, length us, event | category | flops | bytes accessed | tf_op | source)
XLA Modules:
  0.0 268.2 jit_solution(10661251410503181267)
XLA Ops:
  6.5 0.7 all-gather.6.cloned.1.call-update
  7.3 0.7 all-gather.4.cloned.1.call-update
  8.1 0.7 all-gather.8.cloned.1.call-update
  8.8 0.1 copy.50
  9.0 0.2 copy.51
  9.2 0.1 copy.49
  9.3 0.1 copy.52
  9.5 0.1 copy.53.gain_ref
  9.6 0.1 copy.55
  9.7 0.1 reshape.114
  9.9 0.2 convert_reduce_fusion.1
  10.1 0.1 reduce_sum.41
  10.2 0.1 copy.56
  10.3 0.6 dynamic_slice.3
  10.9 49.3 %attend.1 = bf16[8,128,128]{2,1,0:T(8,128)(2,1)S(1)} custom-call(f32[1,1]{1,0:T(1,128)} %bitcast.lam_ref, f32[128,1]{1,0:T(8,128)S(1)} %copy.53.gain_ref, bf16[2,128,512]{2,1,0:T(8,128)(2,1)S(1)} %bitcast.101, bf16[2,512,128]{2,1,0:T(8,128)(2,1)S(1)} %bitcast.100, bf16[2,128,512]{2,1,0:T(8,128)(2,1)S(1)} %bitcast.102), custom_call_target="tpu_custom_call" | custom-call | tf_op jit(solution)/shard_map/attend/pallas_call | solution.py:231
  60.2 0.1 convert_reduce_fusion
  60.3 3.0 %multiply_reduce_fusion.1 = (f32[128]{0:T(128)S(1)}, f32[128,2048]{1,0:T(8,128)S(1)}) fusion(bf16[1024,128]{1,0:T(8,128)(2,1)S(1)} %bitcast.99, bf16[1024,2048]{1,0:T(8,128)(2,1)} %param.18, bf16[128,2048]{1,0:T(8,128)(2,1)S(1)} %copy-done), kind=kOutput, calls=%fused_computation.30 | convolution fusion | flops 538967936 | bytes 6029824 | tf_op jit(solution)/shard_map/dot_general | solution.py:280
  63.3 0.8 fusion.9
  64.1 60.8 %all_to_all.10 = bf16[64,1,8,2048]{3,2,1,0:T(8,128)(2,1)S(1)} all-to-all(bf16[64,1,8,2048]{3,2,1,0:T(8,128)(2,1)S(1)} %fusion.9), channel_id=1, replica_groups=mesh['sp'=64,'tp'=4] {'sp'}, dimensions={0} | all-to-all | bytes 4194304 | tf_op jit(solution)/shard_map/all_to_all | solution.py:307
  124.9 5.8 %fusion.2 = f32[64,8,1024]{2,1,0:T(8,128)} fusion(bf16[1,2048,1024]{2,1,0:T(8,128)(2,1)} %all-gather.6.cloned.1.call-done, bf16[64,1,8,2048]{3,2,1,0:T(8,128)(2,1)S(1)} %all_to_all.10), kind=kOutput, calls=%fused_computation.3 | convolution fusion | flops 2147483648 | bytes 8388608 | tf_op jit(solution)/shard_map/secd,edf->secf/dot_general | solution.py:268
  130.7 50.0 %all-gather.8.cloned.1.call-done = bf16[1,2048,1024]{2,1,0:T(8,128)(2,1)} async-done(((bf16[1,2048,256]{2,1,0:T(8,128)(2,1)}), bf16[1,2048,1024]{2,1,0:T(8,128)(2,1)}) %all-gather.8.cloned.1.call-update) | async-done | bytes 4194320 | tf_op jit(solution)/shard_map/all_gather | solution.py:304
  180.7 10.0 %fusion.10 = bf16[64,1,8,2048]{3,2,1,0:T(8,128)(2,1)} fusion(bf16[1,2048,1024]{2,1,0:T(8,128)(2,1)} %all-gather.8.cloned.1.call-done, f32[64,8,1024]{2,1,0:T(8,128)} %fusion.2, bf16[1,2048,1024]{2,1,0:T(8,128)(2,1)} %all-gather.4.cloned.1.call-done, bf16[64,1,8,2048]{3,2,1,0:T(8,128)(2,1)S(1)} %all_to_all.10), kind=kOutput, calls=%fused_computation.10 | convolution fusion | flops 4299161600 | bytes 14680064 | tf_op jit(solution)/shard_map/secf,edf->secd/dot_general | solution.py:309
  190.7 12.2 %all-to-all-start.1 = ((bf16[64,1,8,2048]{3,2,1,0:T(8,128)(2,1)}), bf16[64,1,8,2048]{3,2,1,0:T(8,128)(2,1)S(1)}, u32[]{:S(2)}, u32[]{:S(2)}) async-start(bf16[64,1,8,2048]{3,2,1,0:T(8,128)(2,1)} %fusion.10), calls=%async_computation.1 | async-start | bytes 4194304 | tf_op jit(solution)/shard_map/all_to_all | solution.py:273
  202.9 0.1 copy.60
  203.0 0.1 mul.73
  203.1 0.1 copy.57
  203.3 0.1 copy.54
  203.4 49.2 %all-to-all-done.1 = bf16[64,1,8,2048]{3,2,1,0:T(8,128)(2,1)S(1)} async-done(((bf16[64,1,8,2048]{3,2,1,0:T(8,128)(2,1)}), bf16[64,1,8,2048]{3,2,1,0:T(8,128)(2,1)S(1)}, u32[]{:S(2)}, u32[]{:S(2)}) %all-to-all-start.1) | async-done | bytes 2097184 | tf_op jit(solution)/shard_map/all_to_all | solution.py:273
  252.6 2.3 gather_fusion
  254.9 1.7 gather.7
  256.7 4.1 %multiply_reduce_fusion = f32[128,2048]{1,0:T(8,128)S(1)} fusion(bf16[128,2,2048]{2,1,0:T(2,128)(2,1)S(1)} %gather.7, pred[128,2]{1,0:T(8,128)(4,1)S(1)} %copy.57, f32[128,2]{1,0:T(8,128)S(1)} %copy.54), kind=kLoop, calls=%fused_computation.25 | loop fusion | flops 1835008 | bytes 2098432 | tf_op jit(solution)/shard_map/reduce_sum | solution.py:313
  260.7 0.9 add_convert_fusion
  (29 shorter events, 0.2 us)
Async XLA Ops:
  6.5 2.3 copy-start.1
  6.5 2.6 copy-start.2
  6.5 118.3 %all-gather.6.cloned.1.call-start = ((), (), s32[]{:S(2)}) async-start(), calls=%async_computation.3 | async-start | bytes 5242880 | tf_op jit(solution)/shard_map/all_gather | solution.py:303
  7.3 2.1 copy-start.3
  7.3 2.2 copy-start.7
  7.3 2.3 copy-start.4
  7.3 3.0 %copy-start.8 = (f32[2]{0:T(128)S(1)}, f32[2]{0:T(128)}, u32[]{:S(2)}) copy-start(f32[2]{0:T(128)} %param.16) | copy-start | bytes 28
  7.3 123.4 %all-gather.4.cloned.1.call-start = ((), (), s32[]{:S(2)}) async-start(), calls=%async_computation.2 | async-start | bytes 5242880 | tf_op jit(solution)/shard_map/all_gather | solution.py:302
  8.0 172.7 %all-gather.8.cloned.1.call-start = ((), (), s32[]{:S(2)}) async-start(), calls=%async_computation.4 | async-start | bytes 5242880 | tf_op jit(solution)/shard_map/all_gather | solution.py:304
  8.8 51.5 %copy-start = (bf16[128,2048]{1,0:T(8,128)(2,1)S(1)}, bf16[128,2048]{1,0:T(8,128)(2,1)}, u32[]{:S(2)}) copy-start(bf16[128,2048]{1,0:T(8,128)(2,1)} %param.19) | copy-start | bytes 1572868
  60.3 3.0 %copy-start.5 = (f32[2048]{0:T(1024)S(1)}, f32[2048]{0:T(1024)}, u32[]{:S(2)}) copy-start(f32[2048]{0:T(1024)} %param.20) | copy-start | bytes 24580
  190.7 12.6 %copy-start.6 = (f32[128,2]{0,1:T(2,128)S(1)}, f32[128,2]{0,1:T(2,128)}, u32[]{:S(2)}) copy-start(f32[128,2]{0,1:T(2,128)} %param.22) | copy-start | bytes 3076
  190.7 61.9 %all-to-all-start.1 = ((bf16[64,1,8,2048]{3,2,1,0:T(8,128)(2,1)}), bf16[64,1,8,2048]{3,2,1,0:T(8,128)(2,1)S(1)}, u32[]{:S(2)}, u32[]{:S(2)}) async-start(bf16[64,1,8,2048]{3,2,1,0:T(8,128)(2,1)} %fusion.10), calls=%async_computation.1 | async-start | bytes 4194304 | tf_op jit(solution)/shard_map/all_to_all | solution.py:273
Sparse Core Ops, SparseCore 0:
  9.1 59.2 all-gather.5
  70.2 53.6 all-gather.3
  125.8 54.8 all-gather.7

commit v2 on v1

--- a/solution.py
+++ b/solution.py
@@ -13,9 +13,77 @@
 MESH = pl.DeviceIdType.MESH
 
 
-def attend_kernel(lam_ref, gain_ref, q_ref, k_ref, v_ref, o_ref,
+class WeightExchange:
+    def __init__(self, s, x, sources, fulls, send, recv):
+        self.s, self.x, self.sources, self.fulls, self.send, self.recv = s, x, sources, fulls, send, recv
+        self.side = x // 2
+        self.home = s % 2 == self.side
+        self.away = s % 2 != self.side
+        self.beside = x + 1 - 2 * (x % 2)
+        self.opposite = 3 - x
+        self.twin = s + 1 - 2 * (s % 2)
+
+    def copy(self, m, source, quarter, sp, tp, idx):
+        return pltpu.make_async_remote_copy(
+            source, self.fulls[m].at[quarter], self.send.at[m, idx], self.recv.at[m, quarter],
+            device_id={"sp": sp, "tp": tp}, device_id_type=MESH)
+
+    def wait(self, m, quarter):
+        self.copy(m, self.fulls[m].at[quarter], quarter, self.twin, self.x, 0).wait_recv()
+
+    def begin(self):
+        @pl.when(self.home)
+        def _():
+            for m, source in enumerate(self.sources):
+                self.copy(m, source.at[0], self.x, self.s, self.beside, 0).start()
+                self.copy(m, source.at[0], self.x, self.twin, self.x, 1).start()
+
+        @pl.when(self.away)
+        def _():
+            for m, source in enumerate(self.sources):
+                self.copy(m, source.at[0], self.x, self.s, self.opposite, 0).start()
+
+    def cross(self, m):
+        @pl.when(self.home)
+        def _():
+            self.wait(m, self.opposite)
+            block = self.fulls[m].at[self.opposite]
+            self.copy(m, block, self.opposite, self.s, self.beside, 2).start()
+            self.copy(m, block, self.opposite, self.twin, self.x, 3).start()
+
+    def near(self, m):
+        @pl.when(self.home)
+        def _():
+            self.wait(m, self.beside)
+            self.copy(m, self.fulls[m].at[self.beside], self.beside, self.twin, self.x, 4).start()
+
+    def far(self, m):
+        quarter = 3 - self.beside
+
+        @pl.when(self.home)
+        def _():
+            self.wait(m, quarter)
+            self.copy(m, self.fulls[m].at[quarter], quarter, self.twin, self.x, 5).start()
+
+    def finish(self):
+        for m in range(len(self.sources)):
+            block = self.sources[m].at[0]
+
+            @pl.when(self.home)
+            def _(m=m, block=block):
+                for idx in range(6):
+                    self.copy(m, block, self.x, self.twin, self.x, idx).wait_send()
+
+            @pl.when(self.away)
+            def _(m=m, block=block):
+                self.copy(m, block, self.x, self.twin, self.x, 0).wait_send()
+                for quarter in range(4):
+                    self.wait(m, quarter)
+
+
+def attend_kernel(lam_ref, gain_ref, q_ref, k_ref, v_ref, wg_ref, wu_ref, o_ref, fg_ref, fu_ref,
                   kbuf, vbuf, qbuf, qz, sbuf, ebuf, acc, mrun, att,
-                  ssem, rsem, qsem, osend, orecv):
+                  ssem, rsem, qsem, osend, orecv, wsend, wrecv):
     s = lax.axis_index("sp")
     x = lax.axis_index("tp")
     rows = q_ref.shape[2]
@@ -79,6 +147,9 @@
     start(pair_copy(k_ref.at[1 - zb], v_ref.at[1 - zb], mine, zpeer, 0))
     start(pair_copy(own_k, own_v, mine, y1dev, 1))
     start(pair_copy(own_k, own_v, mine, y3dev, 2))
+
+    weights = WeightExchange(s, x, (wg_ref, wu_ref), (fg_ref, fu_ref), wsend, wrecv)
+    weights.begin()
 
     kbuf[mine // 2, pl.ds(pl.multiple_of(c * rows, rows), rows), :] = k_ref[zb]
     vbuf[mine, pl.ds(0, 128), :] = v_ref[zb]
@@ -161,6 +232,19 @@
             @pl.when(i == k - 1)
             def _(k=k):
                 comm(k)
+        @pl.when(i == 3)
+        def _():
+            weights.cross(0)
+            weights.near(0)
+
+        @pl.when(i == 5)
+        def _():
+            weights.cross(1)
+            weights.near(1)
+
+        @pl.when(i == 7)
+        def _():
+            weights.far(0)
         j = i // 2
         gray = j + (j // 2) - 2 * (j // 2) * (j % 2)
         lo, hi = gray % 2, gray // 2
@@ -208,16 +292,18 @@
             pltpu.make_async_remote_copy(
                 att.at[0], o_ref.at[hh], osend.at[0], orecv.at[hh],
                 device_id={"sp": zpeer, "tp": x}, device_id_type=MESH).wait_recv()
+    weights.far(1)
     for copy in sends:
         copy.wait_send()
     qcopy.wait_send()
+    weights.finish()
     for idx in range(15):
         a, b = pair_copy(own_k, own_v, mine, twin, idx)
         a.wait_send()
         b.wait_send()
 
 
-def attend(queries, keys, values, lambdas, head_gain):
+def attend(queries, keys, values, lambdas, head_gain, w_gate, w_up):
     rows = queries.shape[0]
     zb = (lax.axis_index("sp") // 8) % 2
     q = jnp.transpose(queries.reshape(rows, 2, 128), (1, 2, 0))
@@ -228,11 +314,13 @@
     bf, f32 = jnp.bfloat16, jnp.float32
     tiles = 4 * rows // 256
     vm = pl.BlockSpec(memory_space=pltpu.VMEM)
+    hbm = pl.BlockSpec(memory_space=pltpu.HBM)
     return pl.pallas_call(
         attend_kernel,
-        out_shape=jax.ShapeDtypeStruct((8, 128, 128), bf),
-        in_specs=[pl.BlockSpec(memory_space=pltpu.SMEM), vm, vm, vm, vm],
-        out_specs=vm,
+        out_shape=(jax.ShapeDtypeStruct((8, 128, 128), bf), jax.ShapeDtypeStruct((4,) + w_gate.shape[1:], bf),
+                   jax.ShapeDtypeStruct((4,) + w_up.shape[1:], bf)),
+        in_specs=[pl.BlockSpec(memory_space=pltpu.SMEM), vm, vm, vm, vm, hbm, hbm],
+        out_specs=(vm, hbm, hbm),
         scratch_shapes=[
             pltpu.VMEM((8, 2 * rows, 128), bf),
             pltpu.VMEM((16, 144, rows), bf),
@@ -248,36 +336,336 @@
             pltpu.SemaphoreType.DMA((2,)),
             pltpu.SemaphoreType.DMA((7,)),
             pltpu.SemaphoreType.DMA((8,)),
+            pltpu.SemaphoreType.DMA((2, 6)),
+            pltpu.SemaphoreType.DMA((2, 4)),
         ],
         compiler_params=pltpu.CompilerParams(collective_id=1, has_side_effects=True,
                                              vmem_limit_bytes=40 * 1024 * 1024),
         name="attend",
-    )(lam, gain, q, k, v)
-
-
-def slot_numbers(flat_ids):
-    count_ids = flat_ids.shape[0]
-    positions = lax.broadcasted_iota(jnp.int32, (count_ids, count_ids), 0)
-    earlier = lax.broadcasted_iota(jnp.int32, (count_ids, count_ids), 1) < positions
-    matches = (flat_ids[:, None] == flat_ids[None, :]) & earlier
-    return jnp.sum(matches.astype(jnp.int32), axis=1)
-
-
-def expert_hidden(arrived, gate_weight, up_weight):
-    gate_proj = jnp.einsum("secd,edf->secf", arrived, gate_weight, preferred_element_type=jnp.float32)
-    up_proj = jnp.einsum("secd,edf->secf", arrived, up_weight, preferred_element_type=jnp.float32)
-    return (jax.nn.silu(gate_proj) * up_proj).astype(jnp.bfloat16)
-
-
-def send_back(results):
-    return lax.all_to_all(results, "sp", split_axis=0, concat_axis=0, tiled=True)
+    )(lam, gain, q, k, v, w_gate, w_up)
+
+
+Z_STEPS = (0, 1, 7, 2, 6, 3, 5, 4)
+
+
+def expert_kernel(tok_in, meta_in, carried_ref, place_ref, fg_ref, fu_ref, wg_ref, wu_ref, wd_ref, o_ref,
+                  tok, meta, ex, er, gw, uw, wd, hb, yb, rb, cb, fin,
+                  tsend, trecv, msend, mrecv, esend, erecv, ysend, yrecv, fsend, frecv, wsem, dsend, drecv):
+    s = lax.axis_index("sp")
+    x = lax.axis_index("tp")
+    z = s // 8
+    y = (s // 2) % 4
+    c = s % 2
+    side = x // 2
+    weights = WeightExchange(s, x, (wd_ref,), (wd,), dsend, drecv)
+
+    def z_device(step):
+        return ((z + step) % 8) * 8 + y * 2 + c
+
+    def expert_of(k):
+        which = k % 2
+        stays = 1 - (which + side - 2 * which * side)
+        return z * 8 + ((y + k // 2) % 4) * 2 + (1 - stays), stays * x + (1 - stays) * (3 - x)
+
+    def expert_number(k):
+        return ((y + k // 2) % 4) * 2 + k % 2
+
+    plane = (1 - c) * x + c * (3 - x)
+
+    def hub_of(h):
+        return z * 8 + hub_number(h), plane
+
+    def hub_number(h):
+        return ((y + h // 2) % 4) * 2 + (c + h) % 2
+
+    my_expert = y * 2 + side
+    other = c == 1
+
+    def self_expert(k):
+        return k // 2 == 0
+
+    def when_remote_expert(k, body):
+        if k // 2 == 0:
+            pl.when(jnp.logical_or(other, side != k % 2))(body)
+        else:
+            body()
+
+    def when_remote_hub(h, body):
+        if h == 0:
+            pl.when(other)(body)
+        else:
+            body()
+
+    barrier = pltpu.get_barrier_semaphore()
+
+    def greet(sp, tp):
+        pl.semaphore_signal(barrier, inc=1, device_id={"sp": sp, "tp": tp}, device_id_type=MESH)
+
+    for step in range(1, 8):
+        greet(z_device(step), x)
+    for k in range(8):
+        when_remote_expert(k, lambda k=k: greet(*expert_of(k)))
+        when_remote_hub(k, lambda k=k: greet(*hub_of(k)))
+    greet(s, weights.beside)
+    greet(s, weights.opposite)
+    greet(weights.twin, x)
+    pl.semaphore_wait(barrier, 24 + 2 * c)
+
+    def token_copies(n):
+        dest = {"sp": z_device(Z_STEPS[n]), "tp": x}
+        return (pltpu.make_async_remote_copy(tok_in.at[n], tok.at[n], tsend.at[n], trecv.at[n],
+                                             device_id=dest, device_id_type=MESH),
+                pltpu.make_async_remote_copy(meta_in.at[n], meta.at[n], msend.at[n], mrecv.at[n],
+                                             device_id=dest, device_id_type=MESH))
+
+    for n in range(1, 8):
+        for copy in token_copies(n):
+            copy.start()
+    weights.begin()
+
+    def load(m, source, target, q, sem):
+        return pltpu.make_async_copy(source, target.at[q], wsem.at[m, sem])
+
+    full_refs, own_refs, targets = (fg_ref, fu_ref), (wg_ref, wu_ref), (gw, uw)
+    for m in range(2):
+        for j in range(4):
+            q = (x + j) % 4
+            if j == 0:
+                @pl.when(weights.home)
+                def _(m=m, q=q):
+                    load(m, own_refs[m].at[0], targets[m], q, 0).start()
+
+                @pl.when(weights.away)
+                def _(m=m, q=q):
+                    load(m, full_refs[m].at[q], targets[m], q, 0).start()
+            else:
+                load(m, full_refs[m].at[q], targets[m], q, j).start()
+
+    @pl.when(weights.home)
+    def _():
+        load(2, wd_ref.at[0], wd, x, 0).start()
+
+    tok[0] = tok_in[0]
+    meta[0] = meta_in[0]
+
+    slot_rows = lax.broadcasted_iota(jnp.int32, (128, 32), 0).astype(jnp.float32)
+
+    def chosen(n):
+        first = slot_rows == meta[n, 0:1, 0:32] + 8.0 * (n % 2)
+        second = slot_rows == meta[n, 1:2, 0:32] + 8.0 * (n % 2)
+        return first, second
+
+    def spread(n):
+        first, second = chosen(n)
+        return jnp.where(jnp.logical_or(first, second), 1.0, 0.0).astype(jnp.bfloat16)
+
+    def expert_copy(p, k):
+        sp, tp = expert_of(k)
+        number = expert_number(k)
+        return pltpu.make_async_remote_copy(
+            ex.at[p, number], er.at[p, y * 2 + c], esend.at[p, k], erecv.at[p, y * 2 + c],
+            device_id={"sp": sp, "tp": tp}, device_id_type=MESH)
+
+    def dispatch(p):
+        for n in (2 * p, 2 * p + 1):
+            if n > 0:
+                for copy in token_copies(n):
+                    copy.wait_recv()
+        even, odd = spread(2 * p), spread(2 * p + 1)
+        for part in range(4):
+            here = pl.ds(part * 512, 512)
+            block = jnp.dot(even, tok[2 * p, :, here], preferred_element_type=jnp.float32)
+            block += jnp.dot(odd, tok[2 * p + 1, :, here], preferred_element_type=jnp.float32)
+            ex[p, :, :, here] = block.astype(jnp.bfloat16).reshape(8, 16, 512)
+        for k in (0, 1, 2, 3, 6, 7, 4, 5):
+            when_remote_expert(k, lambda k=k: expert_copy(p, k).start())
+
+        @pl.when(jnp.logical_not(other))
+        def _():
+            er[p, y * 2] = ex[p, my_expert]
+
+    dispatch(0)
+    dispatch(1)
+    weights.cross(0)
+    weights.near(0)
+    dispatch(2)
+    dispatch(3)
+    weights.far(0)
+
+    for m in range(2):
+        for j in range(4):
+            load(m, own_refs[m].at[0], targets[m], x, j).wait()
+
+    def expert_rows_wait(p):
+        for h in range(8):
+            number = hub_number(h)
+            when_remote_hub(h, lambda number=number: pltpu.make_async_remote_copy(
+                ex.at[p, 0], er.at[p, number], esend.at[p, 0], erecv.at[p, number],
+                device_id={"sp": s, "tp": weights.beside}, device_id_type=MESH).wait_recv())
+
+    def output_copy(p, h):
+        sp, tp = hub_of(h)
+        return pltpu.make_async_remote_copy(
+            yb.at[p, hub_number(h)], rb.at[p, my_expert], ysend.at[p, h], yrecv.at[p, my_expert],
+            device_id={"sp": sp, "tp": tp}, device_id_type=MESH)
+
+    def hidden(half):
+        def one_quarter(q, carry):
+            rows = er[pl.ds(2 * half, 2)].reshape(256, 2048)
+            gate = jnp.dot(rows, gw[q], preferred_element_type=jnp.float32)
+            up = jnp.dot(rows, uw[q], preferred_element_type=jnp.float32)
+            hb[q] = (gate / (1.0 + jnp.exp(-gate)) * up).astype(jnp.bfloat16)
+            return carry
+        lax.fori_loop(0, 4, one_quarter, 0)
+
+    def outputs(half):
+        for part in range(8):
+            here = pl.ds(part * 256, 256)
+            total = None
+            for q in range(4):
+                term = lax.dot_general(hb[q], wd[q, here, :], (((1,), (1,)), ((), ())),
+                                       preferred_element_type=jnp.float32)
+                total = term if total is None else total + term
+            yb[pl.ds(2 * half, 2), :, :, here] = total.astype(jnp.bfloat16).reshape(2, 8, 16, 256)
+
+    def send_back(p):
+        for h in (0, 1, 2, 3, 6, 7, 4, 5):
+            when_remote_hub(h, lambda h=h: output_copy(p, h).start())
+
+        @pl.when(jnp.logical_not(other))
+        def _():
+            rb[p, my_expert] = yb[p, y * 2]
+
+    def final_copy(n):
+        dest = {"sp": z_device(8 - Z_STEPS[n]), "tp": x}
+        return pltpu.make_async_remote_copy(cb.at[n], fin.at[n], fsend.at[n], frecv.at[n],
+                                            device_id=dest, device_id_type=MESH)
+
+    def combine(p):
+        for k in range(8):
+            number = expert_number(k)
+            when_remote_expert(k, lambda number=number: pltpu.make_async_remote_copy(
+                yb.at[p, 0], rb.at[p, number], ysend.at[p, 0], yrecv.at[p, number],
+                device_id={"sp": s, "tp": weights.beside}, device_id_type=MESH).wait_recv())
+        for n in (2 * p, 2 * p + 1):
+            first, second = chosen(n)
+            mix = jnp.where(first, meta[n, 2:3, 0:32], 0.0) + jnp.where(second, meta[n, 3:4, 0:32], 0.0)
+            high = mix.astype(jnp.bfloat16)
+            low = (mix - high.astype(jnp.float32)).astype(jnp.bfloat16)
+            both = jnp.transpose(jnp.concatenate([high, low], axis=0).astype(jnp.float32)).astype(jnp.bfloat16)
+            for part in range(4):
+                here = pl.ds(part * 512, 512)
+                rows = rb[p, :, :, here].reshape(128, 512)
+                value = jnp.dot(both[:, :128], rows, preferred_element_type=jnp.float32)
+                value += jnp.dot(both[:, 128:], rows, preferred_element_type=jnp.float32)
+                cb[n, :, here] = value.astype(jnp.bfloat16)
+            if n > 0:
+                final_copy(n).start()
+
+    for half in range(2):
+        expert_rows_wait(2 * half)
+        expert_rows_wait(2 * half + 1)
+        hidden(half)
+        if half == 0:
+            @pl.when(weights.home)
+            def _():
+                load(2, wd_ref.at[0], wd, x, 0).wait()
+            weights.finish()
+        outputs(half)
+        send_back(2 * half)
+        send_back(2 * half + 1)
+    for p in range(4):
+        combine(p)
+
+    for n in range(1, 8):
+        final_copy(n).wait_recv()
+    fin[0] = cb[0]
+    places = lax.broadcasted_iota(jnp.int32, (128, 256), 1)
+    pick = jnp.where(places == place_ref[...], 1.0, 0.0).astype(jnp.bfloat16)
+    for part in range(4):
+        here = pl.ds(part * 512, 512)
+        value = jnp.dot(pick, fin[:, :, here].reshape(256, 512), preferred_element_type=jnp.float32)
+        o_ref[:, here] = (carried_ref[:, here].astype(jnp.float32) + value).astype(jnp.bfloat16)
+
+    for n in range(1, 8):
+        for copy in token_copies(n):
+            copy.wait_send()
+        final_copy(n).wait_send()
+    for p in range(4):
+        for k in range(8):
+            when_remote_expert(k, lambda k=k: expert_copy(p, k).wait_send())
+            when_remote_hub(k, lambda k=k: output_copy(p, k).wait_send())
+
+
+def experts(grouped, meta, carried, place, full_gate, full_up, w_gate, w_up, w_down):
+    bf, f32 = jnp.bfloat16, jnp.float32
+    vm = pl.BlockSpec(memory_space=pltpu.VMEM)
+    hbm = pl.BlockSpec(memory_space=pltpu.HBM)
+    dma = pltpu.SemaphoreType.DMA
+    return pl.pallas_call(
+        expert_kernel,
+        out_shape=jax.ShapeDtypeStruct((128, 2048), bf),
+        in_specs=[vm, vm, vm, vm, hbm, hbm, hbm, hbm, hbm],
+        out_specs=vm,
+        scratch_shapes=[
+            pltpu.VMEM((8, 32, 2048), bf),
+            pltpu.VMEM((8, 8, 128), f32),
+            pltpu.VMEM((4, 8, 16, 2048), bf),
+            pltpu.VMEM((4, 8, 16, 2048), bf),
+            pltpu.VMEM((4, 2048, 256), bf),
+            pltpu.VMEM((4, 2048, 256), bf),
+            pltpu.VMEM((4, 2048, 256), bf),
+            pltpu.VMEM((4, 256, 256), bf),
+            pltpu.VMEM((4, 8, 16, 2048), bf),
+            pltpu.VMEM((4, 8, 16, 2048), bf),
+            pltpu.VMEM((8, 32, 2048), bf),
+            pltpu.VMEM((8, 32, 2048), bf),
+            dma((8,)), dma((8,)), dma((8,)), dma((8,)),
+            dma((4, 8)), dma((4, 8)), dma((4, 8)), dma((4, 8)),
+            dma((8,)), dma((8,)), dma((3, 4)), dma((1, 6)), dma((1, 4)),
+        ],
+        compiler_params=pltpu.CompilerParams(collective_id=2, has_side_effects=True,
+                                             vmem_limit_bytes=56 * 1024 * 1024),
+        name="experts",
+    )(grouped, meta, carried, place, full_gate, full_up, w_gate, w_up, w_down)
+
+
+def routing(route_ids, route_weight):
+    rows = route_ids.shape[0]
+    z = lax.axis_index("sp") // 8
+    ids = jnp.transpose(route_ids)
+    group = ids[0] // 8
+    earlier = lax.broadcasted_iota(jnp.int32, (rows, rows), 0) < lax.broadcasted_iota(jnp.int32, (rows, rows), 1)
+
+    def count(mask):
+        return jnp.sum((mask & earlier).astype(jnp.int32), axis=0)
+
+    same_first = (route_ids[:, 0:1] == ids[0:1]) | (route_ids[:, 1:2] == ids[0:1])
+    same_second = (route_ids[:, 0:1] == ids[1:2]) | (route_ids[:, 1:2] == ids[1:2])
+    same_group = (route_ids[:, 0:1] // 8) == group[None]
+    slot0, slot1, position = count(same_first), count(same_second), count(same_group)
+    away = (group - z + 8) % 8
+    turn = jnp.where(away == 0, 0, jnp.where(away < 4, 2 * away - 1, 2 * (8 - away)))
+    turn = jnp.where(away == 4, 7, turn)
+    place = turn * 32 + position
+    select = place[None, :] == lax.broadcasted_iota(jnp.int32, (8 * 32, rows), 0)
+    facts = jnp.stack([
+        ((ids[0] % 8) * 16 + slot0 + 1000).astype(jnp.float32),
+        ((ids[1] % 8) * 16 + slot1 + 1000).astype(jnp.float32),
+        route_weight[:, 0], route_weight[:, 1],
+    ])
+    table = jnp.sum(jnp.where(select[None], facts[:, None, :], 0.0), axis=2)
+    table = jnp.concatenate([table[:2] - 1000.0, table[2:]], axis=0)
+    meta = jnp.transpose(table.reshape(4, 8, 32), (1, 0, 2))
+    return place.reshape(rows, 1), select.astype(jnp.bfloat16), jnp.pad(meta, ((0, 0), (0, 4), (0, 96)))
 
 
 def local(queries, keys, values, lambdas, head_gain, w_out, residual_in, norm_gain,
           route_ids, route_weight, w_gate, w_up, w_down):
-    attended = attend(queries, keys, values, lambdas, head_gain).reshape(8 * 128, 128)
-    dev_rows = residual_in.shape[0]
-    mixed_sum = lax.dot_general(attended, w_out, (((0,), (0,)), ((), ())), preferred_element_type=jnp.float32)
+    attended, full_gate, full_up = attend(queries, keys, values, lambdas, head_gain, w_gate, w_up)
+    place, select, meta = routing(route_ids, route_weight)
+    mixed_sum = lax.dot_general(attended.reshape(8 * 128, 128), w_out, (((0,), (0,)), ((), ())),
+                                preferred_element_type=jnp.float32)
     mixed_out = mixed_sum.astype(jnp.bfloat16)
     carried = (residual_in.astype(jnp.float32) + mixed_out.astype(jnp.float32)).astype(jnp.bfloat16)
     carried_wide = carried.astype(jnp.float32)
@@ -286,32 +674,8 @@
         * lax.rsqrt(jnp.mean(carried_wide * carried_wide, axis=-1, keepdims=True) + EPSILON)
         * norm_gain
     ).astype(jnp.bfloat16)
-    model_width = normed.shape[1]
-    experts_here = w_gate.shape[0]
-    expert_count = experts_here * lax.axis_size("sp")
-    capacity = max(2, 4 * dev_rows // expert_count)
-    flat_ids = route_ids.reshape(-1)
-    targets = flat_ids * capacity + slot_numbers(flat_ids)
-    slot_ids = lax.broadcasted_iota(jnp.int32, (expert_count * capacity, dev_rows, 2), 0)
-    placement_matrix = jnp.sum(
-        (targets.reshape(1, dev_rows, 2) == slot_ids).astype(jnp.int32), axis=2
-    ).astype(jnp.bfloat16)
-    outgoing = jnp.dot(placement_matrix, normed, preferred_element_type=jnp.float32).astype(jnp.bfloat16)
-    outgoing = outgoing.reshape(lax.axis_size("sp"), experts_here, capacity, model_width)
-    full_gate, full_up, full_down = (
-        lax.all_gather(w_gate, "tp", axis=2, tiled=True),
-        lax.all_gather(w_up, "tp", axis=2, tiled=True),
-        lax.all_gather(w_down, "tp", axis=2, tiled=True),
-    )
-    hidden_units = expert_hidden(
-        lax.all_to_all(outgoing, "sp", split_axis=0, concat_axis=0, tiled=True), full_gate, full_up
-    )
-    summed = jnp.einsum("secf,edf->secd", hidden_units, full_down, preferred_element_type=jnp.float32)
-    returned = send_back(summed.astype(jnp.bfloat16))
-    flat_back = returned.reshape(expert_count * capacity, model_width)
-    picked = jnp.take(flat_back, targets, axis=0).astype(jnp.float32).reshape(dev_rows, 2, model_width)
-    layer_out = carried_wide + jnp.sum(route_weight[..., None] * picked, axis=1)
-    return layer_out.astype(jnp.bfloat16)
+    grouped = jnp.dot(select, normed, preferred_element_type=jnp.float32).astype(jnp.bfloat16)
+    return experts(grouped.reshape(8, 32, -1), meta, carried, place, full_gate, full_up, w_gate, w_up, w_down)
 
 
 def solution(mesh):

time: 269 us -> 178 us (0.66)
  Pallas kernels: 49.3 us -> 153 us
  waiting for transfers between devices: 101 us -> 0 us
  blocking collectives: 60.8 us -> 0 us
  matrix products: 19.6 us -> 4.61 us
  between operations: 13.4 us -> 0.13 us
  starting transfers between devices: 12.3 us -> 0 us
  local copies, waits for them, and re-layouts: 6.38 us -> 16.4 us
    pallas_call x1 -> x2, Pallas kernels: 49.3 us -> 153 us  [the longest x1 93.2 us: experts(): pl.pallas_call(expert_kernel, out_shape=jax.ShapeDtypeStruct((128, 2048),...]
    all_to_all x1 -> x0, blocking collectives: 60.8 us -> none  [local(): lax.all_to_all(outgoing, 'sp', split_axis=0, concat_axis=0, tiled=True)]
    all_gather x3 -> x0, waiting for transfers between devices: 50 us -> none  [the longest x1 50 us: local(): lax.all_gather(w_down, 'tp', axis=2, tiled=True)]
    all_to_all x1 -> x0, waiting for transfers between devices: 49.2 us -> none  [send_back(): lax.all_to_all(results, 'sp', split_axis=0, concat_axis=0, tiled=True)]
    dot_general x4 -> x2, matrix products: 19.6 us -> 4.61 us  [the longest x1 3.03 us: local(): lax.dot_general(attended.reshape(8 * 128, 128), w_out, (((0,), (0,)), (()...]
    all_to_all x1 -> x0, starting transfers between devices: 12.2 us -> none  [send_back(): lax.all_to_all(results, 'sp', split_axis=0, concat_axis=0, tiled=True)]
    unnamed x23 -> x19, local copies, waits for them, and re-layouts: 0.69 us -> 11.6 us
    gather x2 -> x0, local copies, waits for them, and re-layouts: 4.08 us -> none  [local(): jnp.take(flat_back, targets, axis=0).astype(jnp.float32)]
  transfers between devices with their start and end apart: 4 -> 0, of which waited for: 2 -> 0; matrix products, arithmetic and copies ran while one was open for 5% -> 0% of each run, Pallas kernels for 18% -> 0%
where the time goes in v2:
time: 178 us; the launch traced here: 177 us
  Pallas kernels  153 us (86%)
  local copies, waits for them, and re-layouts  16.4 us (9%)
  matrix products  4.61 us (3%)
  other arithmetic  3.47 us (2%)
    pallas_call x1, Pallas kernels, experts(): pl.pallas_call(expert_kernel, out_shape=jax.ShapeDtypeStruct((128, 2048),...  93.2 us
    pallas_call x1, Pallas kernels, attend(): pl.pallas_call(attend_kernel, out_shape=(jax.ShapeDtypeStruct((8, 128, 12...  59.7 us
    unnamed x19, local copies, waits for them, and re-layouts  11.6 us

profile of v2, /device:TPU:1, one launch (start us, length us, event | category | flops | bytes accessed | tf_op | source)
XLA Modules:
  0.0 177.5 jit_solution(9220199341665590642)
XLA Ops:
  0.0 1.3 dynamic_slice.3
  1.3 0.7 multiply_bitcast_fusion
  2.0 0.8 slice_bitcast_fusion.1
  2.7 0.8 slice_bitcast_fusion.3
  3.5 0.8 fusion.29
  4.2 0.1 convert_reduce_fusion.1
  4.3 0.8 add_convert_fusion.1
  5.1 0.7 and_select_fusion.3
  5.8 0.1 copy.60
  5.9 0.1 fusion.10
  6.1 0.1 convert_reduce_fusion.2
  6.2 0.2 select_reduce_fusion
  6.5 0.1 reshape.214
  6.6 0.6 pad.4.meta_in
  7.2 0.1 copy.59
  7.3 0.1 copy.52.gain_ref
  7.4 0.1 copy.54
  7.5 0.7 multiply_add_fusion.place_ref
  8.2 1.1 copy.48
  9.3 1.1 copy.49
  10.4 0.2 copy.50
  10.6 1.1 copy.51
  11.7 0.0 copy-start.2
  11.7 1.2 copy-done.2
  12.9 1.2 copy-done.3
  14.1 59.7 %attend.1 = (bf16[8,128,128]{2,1,0:T(8,128)(2,1)S(1)}, bf16[4,2048,256]{2,1,0:T(8,128)(2,1)S(1)}, bf16[4,2048,256]{2,1,0:T(8,128)(2,1)S(1)}) custom-call(f32[1,1]{1,0:T(1,128)} %bitcast.4.lam_ref, f32[128,1]{1,0:T(8,128)S(1)} %copy.52.gain_ref, bf16[2,128,512]{2,1,0:T(8,128)(2,1)S(1)} %bitcast.49, bf16[2,512,128]{2,1,0:T(8,128)(2,1)S(1)} %bitcast.50, ...), custom_call_target="tpu_custom_call" | custom-call | tf_op jit(solution)/shard_map/attend/pallas_call | solution.py:318
  73.9 1.9 %copy-done = bf16[4,2048,256]{2,1,0:T(8,128)(2,1)} copy-done((bf16[4,2048,256]{2,1,0:T(8,128)(2,1)}, bf16[4,2048,256]{2,1,0:T(8,128)(2,1)S(1)}, u32[]{:S(2)}) %copy-start) | copy-done | bytes 4194328
  75.8 2.0 %copy-done.1 = bf16[4,2048,256]{2,1,0:T(8,128)(2,1)} copy-done((bf16[4,2048,256]{2,1,0:T(8,128)(2,1)}, bf16[4,2048,256]{2,1,0:T(8,128)(2,1)S(1)}, u32[]{:S(2)}) %copy-start.1) | copy-done | bytes 4194328
  77.8 3.0 %fusion.3 = (f32[128]{0:T(128)S(1)}, bf16[128,2048]{1,0:T(8,128)(2,1)S(1)}) fusion(bf16[1024,128]{1,0:T(8,128)(2,1)S(1)} %bitcast.52, bf16[1024,2048]{1,0:T(8,128)(2,1)} %param.18, bf16[128,2048]{1,0:T(8,128)(2,1)S(1)} %copy-done.5), kind=kOutput, calls=%fused_computation.7 | convolution fusion | flops 538967936 | bytes 5505536 | tf_op jit(solution)/shard_map/dot_general | solution.py:667
  80.9 1.6 convolution_convert_fusion
  82.4 93.2 %experts.1 = bf16[128,2048]{1,0:T(8,128)(2,1)} custom-call(bf16[8,32,2048]{2,1,0:T(8,128)(2,1)} %bitcast.53, f32[8,8,128]{2,1,0:T(8,128)} %pad.4.meta_in, bf16[128,2048]{1,0:T(8,128)(2,1)} %copy-done.4, s32[128,1]{1,0:T(8,128)} %multiply_add_fusion.place_ref, bf16[4,2048,256]{2,1,0:T(8,128)(2,1)} %copy-done, bf16[4,2048,256]{2,1,0:T(8,128)(2,1)} %copy-done.1, ...), custom_call_target="tpu_custom_call" | custom-call | tf_op jit(solution)/shard_map/experts/pallas_call | solution.py:605
  175.6 1.9 %copy.65 = bf16[128,2048]{1,0:T(8,128)(2,1)} copy(bf16[128,2048]{1,0:T(8,128)(2,1)} %experts.1) | data formatting | bytes 1048576
  (16 shorter events, 0.1 us)
Async XLA Ops:
  0.0 77.8 %copy-start.5 = (bf16[128,2048]{1,0:T(8,128)(2,1)S(1)}, bf16[128,2048]{1,0:T(8,128)(2,1)}, u32[]{:S(2)}) copy-start(bf16[128,2048]{1,0:T(8,128)(2,1)} %param.19) | copy-start | bytes 1572868
  11.7 1.2 copy-start.2
  12.9 1.2 copy-start.3
  14.1 66.7 %copy-start.6 = (f32[2048]{0:T(1024)S(1)}, f32[2048]{0:T(1024)}, u32[]{:S(2)}) copy-start(f32[2048]{0:T(1024)} %param.20) | copy-start | bytes 24580
  73.9 1.9 %copy-start = (bf16[4,2048,256]{2,1,0:T(8,128)(2,1)}, bf16[4,2048,256]{2,1,0:T(8,128)(2,1)S(1)}, u32[]{:S(2)}) copy-start(bf16[4,2048,256]{2,1,0:T(8,128)(2,1)S(1)} %get-tuple-element.9.fg_ref) | copy-start | bytes 12582916
  75.8 2.0 %copy-start.1 = (bf16[4,2048,256]{2,1,0:T(8,128)(2,1)}, bf16[4,2048,256]{2,1,0:T(8,128)(2,1)S(1)}, u32[]{:S(2)}) copy-start(bf16[4,2048,256]{2,1,0:T(8,128)(2,1)S(1)} %get-tuple-element.10.fu_ref) | copy-start | bytes 12582916
  80.8 1.6 copy-start.4

commit v3 on v2

v3 whole, which is shorter than its diff:
```python
import functools
import jax
import jax.numpy as jnp
from jax import lax
from jax.experimental import pallas as pl
from jax.experimental.pallas import tpu as pltpu
from jax.sharding import PartitionSpec as P

EPSILON = 1e-06
OUT_SCALE = 0.8
FLOOR_SCORE = -1e30
LOG2E = 1.4426950408889634
MESH = pl.DeviceIdType.MESH


class WeightExchange:
    def __init__(self, s, x, places, send, recv):
        self.s, self.x, self.places, self.send, self.recv = s, x, places, send, recv
        self.side = x // 2
        self.home = s % 2 == self.side
        self.away = s % 2 != self.side
        self.beside = x + 1 - 2 * (x % 2)
        self.opposite = 3 - x
        self.twin = s + 1 - 2 * (s % 2)

    def copy(self, m, source, quarter, sp, tp, idx):
        return pltpu.make_async_remote_copy(
            source, self.places[m][quarter], self.send.at[m, idx], self.recv.at[m, quarter],
            device_id={"sp": sp, "tp": tp}, device_id_type=MESH)

    def wait(self, m, quarter):
        self.copy(m, self.places[m][quarter], quarter, self.twin, self.x, 0).wait_recv()

    def share(self, m, quarter, source=None):
        source = self.places[m][quarter] if source is None else source
        self.copy(m, source, quarter, self.twin, self.x, 2 + quarter).start()

    def begin(self, m, source):
        @pl.when(self.home)
        def _():
            self.copy(m, source, 1, self.s, self.beside, 0).start()
            self.share(m, 0, source)

        @pl.when(self.away)
        def _():
            self.copy(m, source, 2, self.s, self.opposite, 0).start()

    def pass_on(self, m, block=None):
        @pl.when(self.home)
        def _():
            self.copy(m, self.places[m][2] if block is None else block, 3, self.s, self.beside, 1).start()

    def landed(self, m, quarter):
        @pl.when(self.home)
        def _():
            self.wait(m, quarter)
            self.share(m, quarter)

    def finish(self, m, source, quarters):
        @pl.when(self.home)
        def _():
            if 1 in quarters:
                self.copy(m, source, 1, self.s, self.beside, 0).wait_send()
            if 3 in quarters:
                self.copy(m, source, 3, self.s, self.beside, 1).wait_send()
            for quarter in quarters:
                self.copy(m, source, quarter, self.twin, self.x, 2 + quarter).wait_send()

        @pl.when(self.away)
        def _():
            if 2 in quarters:
                self.copy(m, source, 2, self.s, self.opposite, 0).wait_send()
            for quarter in quarters:
                self.wait(m, quarter)


def attend_kernel(lam_ref, gain_ref, q_in, k_in, v_in, wout_hbm, res_ref, ngain_ref, ids_ref, rw_ref, wg_ref, wu_ref,
                  group_ref, facts_out, carried_ref, place_ref, fg_ref, fu_ref,
                  q_ref, v_ref, kbuf, vbuf, qbuf, qz, sbuf, ebuf, acc, mrun, att, o_ref, wout, facts,
                  ssem, rsem, qsem, osend, orecv, wsend, wrecv, lsem):
    s = lax.axis_index("sp")
    x = lax.axis_index("tp")
    rows = q_in.shape[0]
    zb = (s // 8) % 2
    y = (s // 2) % 4
    c = s % 2
    mine = s % 16
    base = s - mine
    y1 = y + 1 - 2 * (y % 2)
    y3 = 3 - y
    y2 = (y + 2) % 4

    def slot_of(zz, yy, cc):
        return zz * 8 + yy * 2 + cc

    zpeer = base + slot_of(1 - zb, y, c)
    y1dev = base + slot_of(zb, y1, c)
    y3dev = base + slot_of(zb, y3, c)
    twin = base + slot_of(zb, y, 1 - c)

    barrier = pltpu.get_barrier_semaphore()
    peers = [(zpeer, x), (y1dev, x), (y3dev, x), (twin, x)]
    for j in range(1, 4):
        peers.append((s, (x + j) % 4))
        peers.append((zpeer, (x + j) % 4))
    for ps, px in peers:
        pl.semaphore_signal(barrier, inc=1, device_id={"sp": ps, "tp": px}, device_id_type=MESH)
    for b in range(2):
        q_ref[b] = jnp.transpose(q_in[:, 128 * b:128 * (b + 1)])
        v_ref[b] = jnp.transpose(v_in[:, 128 * b:128 * (b + 1)])
    out_load = pltpu.make_async_copy(wout_hbm, wout, lsem.at[0])
    out_load.start()
    own_loads = (pltpu.make_async_copy(wg_ref.at[0], fg_ref.at[0], lsem.at[1]),
                 pltpu.make_async_copy(wu_ref.at[0], fu_ref.at[0], lsem.at[2]))
    pl.semaphore_wait(barrier, len(peers))

    def kslot(slot):
        return kbuf.at[slot // 2, pl.ds(pl.multiple_of((slot % 2) * rows, rows), rows)]

    def vslot(slot):
        return vbuf.at[slot, pl.ds(0, 128)]

    def pair_copy(ksrc, vsrc, slot, dest, idx):
        return (
            pltpu.make_async_remote_copy(ksrc, kslot(slot), ssem.at[idx, 0], rsem.at[slot, 0],
                                         device_id={"sp": dest, "tp": x}, device_id_type=MESH),
            pltpu.make_async_remote_copy(vsrc, vslot(slot), ssem.at[idx, 1], rsem.at[slot, 1],
                                         device_id={"sp": dest, "tp": x}, device_id_type=MESH),
        )

    def start(pair):
        pair[0].start()
        pair[1].start()

    def forward(slot, dest, idx):
        start(pair_copy(kslot(slot), vslot(slot), slot, dest, idx))

    def wait_slot(slot):
        a, b = pair_copy(kslot(slot), vslot(slot), slot, twin, 0)
        a.wait_recv()
        b.wait_recv()

    qcopy = pltpu.make_async_remote_copy(q_ref.at[1 - zb], qbuf, qsem.at[0], qsem.at[1],
                                         device_id={"sp": zpeer, "tp": x}, device_id_type=MESH)
    qcopy.start()

    def key_columns(b):
        return k_in.at[:, pl.ds(pl.multiple_of(b * 128, 128), 128)]

    own_k, own_v = key_columns(zb), v_ref.at[zb]
    start(pair_copy(own_k, own_v, mine, twin, 3))
    start(pair_copy(key_columns(1 - zb), v_ref.at[1 - zb], mine, zpeer, 0))
    start(pair_copy(own_k, own_v, mine, y1dev, 1))
    start(pair_copy(own_k, own_v, mine, y3dev, 2))

    weights = WeightExchange(s, x, ([fg_ref.at[i] for i in range(4)], [fu_ref.at[i] for i in range(3)]), wsend, wrecv)
    weights.begin(0, wg_ref.at[0])
    weights.begin(1, wu_ref.at[0])
    for own in own_loads:
        pl.when(weights.home)(own.start)

    kbuf[mine // 2, pl.ds(pl.multiple_of(c * rows, rows), rows), :] = key_columns(zb)[...]
    vbuf[mine, pl.ds(0, 128), :] = v_ref[zb]
    for slot in range(16):
        vbuf[slot, pl.ds(128, 16), :] = jnp.ones((16, rows), jnp.bfloat16)
    zeros = jnp.zeros((64, rows), jnp.bfloat16)

    def put_queries(value, column):
        qz[pl.ds(0, 64), pl.ds(column, rows)] = value[:64]
        qz[pl.ds(64, 64), pl.ds(column, rows)] = zeros
        qz[pl.ds(0, 64), pl.ds(2 * rows + column, rows)] = zeros
        qz[pl.ds(64, 64), pl.ds(2 * rows + column, rows)] = value[64:]

    put_queries(q_ref[zb], 0)
    mrun[...] = jnp.full(mrun.shape, FLOOR_SCORE, jnp.float32)
    acc[...] = jnp.zeros(acc.shape, jnp.float32)
    routing(z_of(s), ids_ref, rw_ref, facts, place_ref)
    qcopy.wait_recv()
    put_queries(qbuf[...], rows)

    scale = LOG2E * 64 ** (-0.5)
    keys_here = 2 * rows
    tiles = 2 * 2 * rows // 256
    per_map = tiles // 2

    def scores(p, t):
        column = t * 256
        top = None
        for part in range(2):
            value = jnp.dot(kbuf[p, pl.ds(part * rows, rows), :], qz[:, pl.ds(column, 256)],
                            preferred_element_type=jnp.float32)
            sbuf[t % 2, pl.ds(part * rows, rows), :] = value
            peak = jnp.max(value.reshape(rows // 8, 8, 256), axis=0)
            top = peak if top is None else jnp.maximum(top, peak)
        return jnp.max(top, axis=0, keepdims=True) * scale

    def weigh(t, peak):
        old = mrun[t]
        new = jnp.maximum(old, peak)
        mrun[t] = new
        for part in range(4):
            here = pl.ds(part * keys_here // 4, keys_here // 4)
            ebuf[t % 2, here, :] = jnp.exp2(sbuf[t % 2, here, :] * scale - new).astype(jnp.bfloat16)
        return jnp.exp2(old - new)

    def gather_values(p, t, shrink):
        product = jnp.dot(vbuf[2 * p], ebuf[t % 2, pl.ds(0, rows), :], preferred_element_type=jnp.float32)
        product += jnp.dot(vbuf[2 * p + 1], ebuf[t % 2, pl.ds(rows, rows), :], preferred_element_type=jnp.float32)
        acc[t] = acc[t] * shrink + product

    def compute(p):
        peak = scores(p, 0)
        for t in range(tiles):
            following = scores(p, t + 1) if t + 1 < tiles else None
            shrink = weigh(t, peak)
            gather_values(p, t, shrink)
            peak = following

    order = [(0, y), (1, y), (0, y1), (1, y1), (0, y3), (1, y3), (0, y2), (1, y2)]

    def comm(i):
        flip, yy = order[i]
        zz = zb + flip - 2 * zb * flip
        slot = slot_of(zz, yy, c)
        wait_slot(slot)
        if i == 1:
            forward(slot, y1dev, 4)
            forward(slot, y3dev, 5)
        if i == 2:
            forward(slot, y3dev, 8)
        if i == 5:
            forward(slot, y1dev, 12)
        forward(slot, twin, {1: 6, 2: 7, 3: 9, 4: 10, 5: 11, 6: 13, 7: 14}[i])

    def step(i, carry):
        @pl.when(i == 1)
        def _():
            comm(1)
            comm(2)
        for k in range(3, 8):
            @pl.when(i == k - 1)
            def _(k=k):
                comm(k)
        @pl.when(i == 3)
        def _():
            pl.when(weights.home)(lambda: weights.wait(0, 2))
            weights.pass_on(0)
            pl.when(weights.home)(lambda: weights.share(0, 2))
            weights.landed(0, 1)

        @pl.when(i == 5)
        def _():
            weights.landed(1, 2)

        @pl.when(i == 6)
        def _():
            weights.landed(1, 1)
        j = i // 2
        gray = j + (j // 2) - 2 * (j // 2) * (j % 2)
        lo, hi = gray % 2, gray // 2
        yhi, ylo = y // 2, y % 2
        yy = 2 * (yhi + hi - 2 * yhi * hi) + (ylo + lo - 2 * ylo * lo)
        flip = i % 2
        zz = zb + flip - 2 * zb * flip
        wait_slot(slot_of(zz, yy, 1 - c))
        compute(zz * 4 + yy)
        return carry

    lax.fori_loop(0, 8, step, 0)

    lam = lam_ref[0, zb]
    gain = jnp.transpose(jnp.broadcast_to(gain_ref[...], (128, 128)))[:, 0:1]
    head = 2 * x + zb

    def head_columns(hh):
        return o_ref.at[:, pl.ds(pl.multiple_of(hh * 128, 128), 128)]

    for qt in (2, 3, 0, 1):
        first, second = acc[qt], acc[per_map + qt]
        combined = first[:128] / first[128:129] - lam * (second[:128] / second[128:129])
        mean_square = jnp.mean(combined * combined, axis=0, keepdims=True)
        value = combined * lax.rsqrt(mean_square + EPSILON) * gain * OUT_SCALE
        att[2 * qt] = jnp.transpose(value[:, :128]).astype(jnp.bfloat16)
        att[2 * qt + 1] = jnp.transpose(value[:, 128:]).astype(jnp.bfloat16)

    sends = []
    for j in range(4):
        xx = (x + j) % 4
        sends.append(pltpu.make_async_remote_copy(
            att.at[4 + xx], head_columns(head), osend.at[j], orecv.at[head],
            device_id={"sp": zpeer, "tp": xx}, device_id_type=MESH))
        sends[-1].start()
    for j in range(1, 4):
        xx = (x + j) % 4
        sends.append(pltpu.make_async_remote_copy(
            att.at[xx], head_columns(head), osend.at[3 + j], orecv.at[head],
            device_id={"sp": s, "tp": xx}, device_id_type=MESH))
        sends[-1].start()
    head_columns(head)[...] = att[x]
    weights.landed(0, 3)
    out_load.wait()
    for j in range(4):
        xx = (x + j) % 4
        for far in range(2):
            if j == 0 and far == 0:
                continue
            hh = 2 * xx + (1 - zb if far else zb)
            pltpu.make_async_remote_copy(
                att.at[0], head_columns(hh), osend.at[0], orecv.at[hh],
                device_id={"sp": zpeer, "tp": x}, device_id_type=MESH).wait_recv()

    square = jnp.zeros((128, 1), jnp.float32)
    for part in range(4):
        here = pl.ds(part * 512, 512)
        mixed = jnp.dot(o_ref[...], wout[:, here], preferred_element_type=jnp.float32).astype(jnp.bfloat16)
        carried = (res_ref[:, here].astype(jnp.float32) + mixed.astype(jnp.float32)).astype(jnp.bfloat16)
        carried_ref[:, here] = carried
        wide = carried.astype(jnp.float32)
        square += jnp.sum(wide * wide, axis=1, keepdims=True)
    level = lax.rsqrt(square * (1.0 / 2048) + EPSILON)
    numbers = lax.broadcasted_iota(jnp.int32, (128, 256), 1)
    pick = jnp.transpose(jnp.where(numbers == place_ref[...], 1.0, 0.0)).astype(jnp.bfloat16)
    for part in range(4):
        here = pl.ds(part * 512, 512)
        normed = (carried_ref[:, here].astype(jnp.float32) * level * ngain_ref[:, here]).astype(jnp.bfloat16)
        tokens = jnp.dot(pick, normed, preferred_element_type=jnp.float32)
        group_ref[:, :, here] = tokens.astype(jnp.bfloat16).reshape(8, 32, 512)
    facts_out[...] = jnp.dot(pick, facts[...], preferred_element_type=jnp.float32).astype(jnp.bfloat16).reshape(8, 32, 128)

    for copy in sends:
        copy.wait_send()
    qcopy.wait_send()
    for own in own_loads:
        pl.when(weights.home)(own.wait)
    weights.finish(0, wg_ref.at[0], (0, 1, 2, 3))
    weights.finish(1, wu_ref.at[0], (0, 1, 2))
    for idx in range(15):
        a, b = pair_copy(own_k, own_v, mine, twin, idx)
        a.wait_send()
        b.wait_send()


def z_of(s):
    return s // 8


def routing(z, ids_ref, rw_ref, facts, place_ref):
    ids = ids_ref[...]
    first, second = ids[:, 0:1], ids[:, 1:2]
    both = jnp.concatenate([jnp.broadcast_to(first, (128, 128)), jnp.broadcast_to(second, (128, 128))], axis=1)
    turned = jnp.transpose(both.astype(jnp.float32)).astype(jnp.int32)
    first_row, second_row = turned[:128], turned[128:]
    earlier = lax.broadcasted_iota(jnp.int32, (128, 128), 1) < lax.broadcasted_iota(jnp.int32, (128, 128), 0)

    def count(mask):
        return jnp.sum(jnp.where(jnp.logical_and(mask, earlier), 1.0, 0.0), axis=1, keepdims=True).astype(jnp.int32)

    slot0 = count(jnp.logical_or(first_row == first, second_row == first))
    slot1 = count(jnp.logical_or(first_row == second, second_row == second))
    group = lax.shift_right_logical(first, 3)
    position = count(lax.shift_right_logical(first_row, 3) == group)
    away = (group - z + 8) & 7
    turn = jnp.where(away == 0, 0, jnp.where(away < 4, 2 * away - 1, 2 * (8 - away)))
    turn = jnp.where(away == 4, 7, turn)
    place_ref[...] = turn * 32 + position
    row0 = ((first & 7) * 16 + slot0).astype(jnp.float32)
    row1 = ((second & 7) * 16 + slot1).astype(jnp.float32)
    w0, w1 = rw_ref[:, 0:1], rw_ref[:, 1:2]
    h0, h1 = w0.astype(jnp.bfloat16).astype(jnp.float32), w1.astype(jnp.bfloat16).astype(jnp.float32)
    lane = lax.broadcasted_iota(jnp.int32, (128, 128), 1)
    table = jnp.zeros((128, 128), jnp.float32)
    for n, column in enumerate((row0, row1, h0, w0 - h0, h1, w1 - h1)):
        table = jnp.where(lane == n, column, table)
    facts[...] = table.astype(jnp.bfloat16)


def attend(queries, keys, values, lambdas, head_gain, w_out, residual_in, norm_gain, route_ids, route_weight, w_gate, w_up):
    rows = queries.shape[0]
    bf, f32 = jnp.bfloat16, jnp.float32
    tiles = 4 * rows // 256
    vm = pl.BlockSpec(memory_space=pltpu.VMEM)
    hbm = pl.BlockSpec(memory_space=pltpu.HBM)
    dma = pltpu.SemaphoreType.DMA
    return pl.pallas_call(
        attend_kernel,
        out_shape=(jax.ShapeDtypeStruct((8, 32, 2048), bf), jax.ShapeDtypeStruct((8, 32, 128), bf),
                   jax.ShapeDtypeStruct((128, 2048), bf), jax.ShapeDtypeStruct((128, 1), jnp.int32),
                   jax.ShapeDtypeStruct((4,) + w_gate.shape[1:], bf), jax.ShapeDtypeStruct((3,) + w_up.shape[1:], bf)),
        in_specs=[pl.BlockSpec(memory_space=pltpu.SMEM), vm, vm, vm, vm, hbm, vm, vm, vm, vm, hbm, hbm],
        out_specs=(vm, vm, vm, vm, vm, vm),
        scratch_shapes=[
            pltpu.VMEM((2, 128, rows), bf),
            pltpu.VMEM((2, 128, rows), bf),
            pltpu.VMEM((8, 2 * rows, 128), bf),
            pltpu.VMEM((16, 144, rows), bf),
            pltpu.VMEM((128, rows), bf),
            pltpu.VMEM((128, 4 * rows), bf),
            pltpu.VMEM((2, 2 * rows, 256), f32),
            pltpu.VMEM((2, 2 * rows, 256), bf),
            pltpu.VMEM((tiles, 144, 256), f32),
            pltpu.VMEM((tiles, 1, 256), f32),
            pltpu.VMEM((8, 128, 128), bf),
            pltpu.VMEM((128, 1024), bf),
            pltpu.VMEM((1024, 2048), bf),
            pltpu.VMEM((128, 128), bf),
            dma((15, 2)), dma((16, 2)), dma((2,)), dma((7,)), dma((8,)), dma((2, 6)), dma((2, 4)), dma((3,)),
        ],
        compiler_params=pltpu.CompilerParams(collective_id=1, has_side_effects=True,
                                             vmem_limit_bytes=48 * 1024 * 1024),
        name="attend",
    )(lambdas.reshape(1, 2), head_gain.reshape(1, 128), queries, keys, values, w_out, residual_in,
      norm_gain.reshape(1, -1), route_ids, route_weight, w_gate, w_up)


Z_STEPS = (0, 1, 7, 2, 6, 3, 5, 4)


def expert_kernel(tok_in, meta_in, place_ref, fg_ref, fu_ref, wd_ref, o_ref,
                  tok, meta, ex, er, ufar, wd, hb, yb, rb, cb, fin,
                  tsend, trecv, msend, mrecv, esend, erecv, ysend, yrecv, fsend, frecv, wsem, dsend, drecv):
    s = lax.axis_index("sp")
    x = lax.axis_index("tp")
    z = s // 8
    y = (s // 2) % 4
    c = s % 2
    side = x // 2
    weights = WeightExchange(s, x, ([None, None, None, ufar], [wd.at[i] for i in range(4)]), dsend, drecv)
    own_down = wd_ref.at[0]

    def z_device(step):
        return ((z + step) % 8) * 8 + y * 2 + c

    def expert_of(k):
        which = k % 2
        stays = 1 - (which + side - 2 * which * side)
        return z * 8 + ((y + k // 2) % 4) * 2 + (1 - stays), stays * x + (1 - stays) * (3 - x)

    def expert_number(k):
        return ((y + k // 2) % 4) * 2 + k % 2

    plane = (1 - c) * x + c * (3 - x)

    def hub_of(h):
        return z * 8 + hub_number(h), plane

    def hub_number(h):
        return ((y + h // 2) % 4) * 2 + (c + h) % 2

    my_expert = y * 2 + side
    other = c == 1

    def self_expert(k):
        return k // 2 == 0

    def when_remote_expert(k, body):
        if k // 2 == 0:
            pl.when(jnp.logical_or(other, side != k % 2))(body)
        else:
            body()

    def when_remote_hub(h, body):
        if h == 0:
            pl.when(other)(body)
        else:
            body()

    barrier = pltpu.get_barrier_semaphore()

    def greet(sp, tp):
        pl.semaphore_signal(barrier, inc=1, device_id={"sp": sp, "tp": tp}, device_id_type=MESH)

    for step in range(1, 8):
        greet(z_device(step), x)
    for k in range(8):
        when_remote_expert(k, lambda k=k: greet(*expert_of(k)))
        when_remote_hub(k, lambda k=k: greet(*hub_of(k)))
    greet(s, weights.beside)
    greet(s, weights.opposite)
    greet(weights.twin, x)
    pl.semaphore_wait(barrier, 24 + 2 * c)

    def token_copies(n):
        dest = {"sp": z_device(Z_STEPS[n]), "tp": x}
        return (pltpu.make_async_remote_copy(tok_in.at[n], tok.at[n], tsend.at[n], trecv.at[n],
                                             device_id=dest, device_id_type=MESH),
                pltpu.make_async_remote_copy(meta_in.at[n], meta.at[n], msend.at[n], mrecv.at[n],
                                             device_id=dest, device_id_type=MESH))

    for n in range(1, 8):
        for copy in token_copies(n):
            copy.start()
    weights.pass_on(0, fu_ref.at[2])
    weights.begin(1, own_down)
    own_load = pltpu.make_async_copy(own_down, wd.at[0], wsem.at[0])
    pl.when(weights.home)(own_load.start)

    tok[0] = tok_in[0]
    meta[0] = meta_in[0]

    row_lanes = lax.broadcasted_iota(jnp.int32, (32, 128), 1).astype(jnp.float32)

    def fact(n, lane):
        return meta[n, :, lane:lane + 1].astype(jnp.float32)

    def chosen(n):
        return row_lanes == fact(n, 0) + 8.0 * (n % 2), row_lanes == fact(n, 1) + 8.0 * (n % 2)

    def spread(n):
        first, second = chosen(n)
        return jnp.transpose(jnp.where(jnp.logical_or(first, second), 1.0, 0.0)).astype(jnp.bfloat16)

    def expert_copy(p, k):
        sp, tp = expert_of(k)
        number = expert_number(k)
        return pltpu.make_async_remote_copy(
            ex.at[p, number], er.at[p, y * 2 + c], esend.at[p, k], erecv.at[p, y * 2 + c],
            device_id={"sp": sp, "tp": tp}, device_id_type=MESH)

    def dispatch(p):
        for n in (2 * p, 2 * p + 1):
            if n > 0:
                for copy in token_copies(n):
                    copy.wait_recv()
        even, odd = spread(2 * p), spread(2 * p + 1)
        for part in range(4):
            here = pl.ds(part * 512, 512)
            block = jnp.dot(even, tok[2 * p, :, here], preferred_element_type=jnp.float32)
            block += jnp.dot(odd, tok[2 * p + 1, :, here], preferred_element_type=jnp.float32)
            ex[p, :, :, here] = block.astype(jnp.bfloat16).reshape(8, 16, 512)
        for k in (0, 1, 2, 3, 6, 7, 4, 5):
            when_remote_expert(k, lambda k=k: expert_copy(p, k).start())

        @pl.when(jnp.logical_not(other))
        def _():
            er[p, y * 2] = ex[p, my_expert]

    def expert_rows_wait(p):
        for h in range(8):
            number = hub_number(h)
            when_remote_hub(h, lambda number=number: pltpu.make_async_remote_copy(
                ex.at[p, 0], er.at[p, number], esend.at[p, 0], erecv.at[p, number],
                device_id={"sp": s, "tp": weights.beside}, device_id_type=MESH).wait_recv())

    def output_copy(p, h):
        sp, tp = hub_of(h)
        return pltpu.make_async_remote_copy(
            yb.at[p, hub_number(h)], rb.at[p, my_expert], ysend.at[p, h], yrecv.at[p, my_expert],
            device_id={"sp": sp, "tp": tp}, device_id_type=MESH)

    def hidden(half):
        def one_quarter(q, carry):
            unit(q, fu_ref[q])
            return carry

        def unit(q, up_weight):
            rows = er[pl.ds(2 * half, 2)].reshape(256, 2048)
            gate = jnp.dot(rows, fg_ref[q], preferred_element_type=jnp.float32)
            up = jnp.dot(rows, up_weight, preferred_element_type=jnp.float32)
            hb[q] = (gate / (1.0 + jnp.exp(-gate)) * up).astype(jnp.bfloat16)

        lax.fori_loop(0, 3, one_quarter, 0)
        if half == 0:
            weights.landed(0, 3)
            weights.finish(0, own_down, (3,))
        unit(3, ufar[...])

    def outputs(half):
        for part in range(8):
            here = pl.ds(part * 256, 256)
            total = None
            for q in range(4):
                term = lax.dot_general(hb[q], wd[q, here, :], (((1,), (1,)), ((), ())),
                                       preferred_element_type=jnp.float32)
                total = term if total is None else total + term
            yb[pl.ds(2 * half, 2), :, :, here] = total.astype(jnp.bfloat16).reshape(2, 8, 16, 256)

    def send_back(p):
        for h in (0, 1, 2, 3, 6, 7, 4, 5):
            when_remote_hub(h, lambda h=h: output_copy(p, h).start())

        @pl.when(jnp.logical_not(other))
        def _():
            rb[p, my_expert] = yb[p, y * 2]

    def final_copy(n):
        dest = {"sp": z_device(8 - Z_STEPS[n]), "tp": x}
        return pltpu.make_async_remote_copy(cb.at[n], fin.at[n], fsend.at[n], frecv.at[n],
                                            device_id=dest, device_id_type=MESH)

    def combine(p):
        for k in range(8):
            number = expert_number(k)
            when_remote_expert(k, lambda number=number: pltpu.make_async_remote_copy(
                yb.at[p, 0], rb.at[p, number], ysend.at[p, 0], yrecv.at[p, number],
                device_id={"sp": s, "tp": weights.beside}, device_id_type=MESH).wait_recv())
        for n in (2 * p, 2 * p + 1):
            first, second = chosen(n)
            high = jnp.where(first, fact(n, 2), 0.0) + jnp.where(second, fact(n, 4), 0.0)
            low = jnp.where(first, fact(n, 3), 0.0) + jnp.where(second, fact(n, 5), 0.0)
            high, low = high.astype(jnp.bfloat16), low.astype(jnp.bfloat16)
            for part in range(4):
                here = pl.ds(part * 512, 512)
                rows = rb[p, :, :, here].reshape(128, 512)
                value = jnp.dot(high, rows, preferred_element_type=jnp.float32)
                value += jnp.dot(low, rows, preferred_element_type=jnp.float32)
                cb[n, :, here] = value.astype(jnp.bfloat16)
            if n > 0:
                final_copy(n).start()

    dispatch(0)
    dispatch(1)
    weights.landed(1, 2)
    weights.pass_on(1)
    dispatch(2)
    expert_rows_wait(0)
    expert_rows_wait(1)
    hidden(0)
    dispatch(3)
    pl.when(weights.home)(own_load.wait)
    weights.landed(1, 1)
    weights.landed(1, 3)
    weights.finish(1, own_down, (0, 1, 2, 3))
    outputs(0)
    send_back(0)
    send_back(1)
    expert_rows_wait(2)
    expert_rows_wait(3)
    hidden(1)
    outputs(1)
    send_back(2)
    send_back(3)
    for p in range(4):
        combine(p)

    for n in range(1, 8):
        final_copy(n).wait_recv()
    fin[0] = cb[0]
    places = lax.broadcasted_iota(jnp.int32, (128, 256), 1)
    pick = jnp.where(places == place_ref[...], 1.0, 0.0).astype(jnp.bfloat16)
    for part in range(4):
        here = pl.ds(part * 512, 512)
        value = jnp.dot(pick, fin[:, :, here].reshape(256, 512), preferred_element_type=jnp.float32)
        o_ref[:, here] = value

    for n in range(1, 8):
        for copy in token_copies(n):
            copy.wait_send()
        final_copy(n).wait_send()
    for p in range(4):
        for k in range(8):
            when_remote_expert(k, lambda k=k: expert_copy(p, k).wait_send())
            when_remote_hub(k, lambda k=k: output_copy(p, k).wait_send())


def experts(grouped, facts, place, full_gate, full_up, w_down):
    bf, f32 = jnp.bfloat16, jnp.float32
    vm = pl.BlockSpec(memory_space=pltpu.VMEM)
    hbm = pl.BlockSpec(memory_space=pltpu.HBM)
    dma = pltpu.SemaphoreType.DMA
    return pl.pallas_call(
        expert_kernel,
        out_shape=jax.ShapeDtypeStruct((128, 2048), f32),
        in_specs=[vm, vm, vm, vm, vm, hbm],
        out_specs=vm,
        scratch_shapes=[
            pltpu.VMEM((8, 32, 2048), bf),
            pltpu.VMEM((8, 32, 128), bf),
            pltpu.VMEM((4, 8, 16, 2048), bf),
            pltpu.VMEM((4, 8, 16, 2048), bf),
            pltpu.VMEM((2048, 256), bf),
            pltpu.VMEM((4, 2048, 256), bf),
            pltpu.VMEM((4, 256, 256), bf),
            pltpu.VMEM((4, 8, 16, 2048), bf),
            pltpu.VMEM((4, 8, 16, 2048), bf),
            pltpu.VMEM((8, 32, 2048), bf),
            pltpu.VMEM((8, 32, 2048), bf),
            dma((8,)), dma((8,)), dma((8,)), dma((8,)),
            dma((4, 8)), dma((4, 8)), dma((4, 8)), dma((4, 8)),
            dma((8,)), dma((8,)), dma((1,)), dma((2, 6)), dma((2, 4)),
        ],
        compiler_params=pltpu.CompilerParams(collective_id=2, has_side_effects=True,
                                             vmem_limit_bytes=46 * 1024 * 1024),
        name="experts",
    )(grouped, facts, place, full_gate, full_up, w_down)


def local(queries, keys, values, lambdas, head_gain, w_out, residual_in, norm_gain,
          route_ids, route_weight, w_gate, w_up, w_down):
    grouped, facts, carried, place, full_gate, full_up = attend(
        queries, keys, values, lambdas, head_gain, w_out, residual_in, norm_gain, route_ids, route_weight, w_gate, w_up)
    mixture = experts(grouped, facts, place, full_gate, full_up, w_down)
    return (carried.astype(jnp.float32) + mixture).astype(jnp.bfloat16)


def solution(mesh):
    placed = (
        P("sp", "tp"), P("sp", "tp"), P("sp", "tp"), P("tp"), P(), P(),
        P(("sp", "tp"), None), P(), P(("sp", "tp"), None), P(("sp", "tp"), None),
        P("sp", None, "tp"), P("sp", None, "tp"), P("sp", None, "tp"),
    )
    return jax.shard_map(local, mesh=mesh, in_specs=placed, out_specs=P(("sp", "tp"), None), check_vma=False)
```

time: 178 us -> 161 us (0.904)
  Pallas kernels: 153 us -> 147 us
  matrix products: 4.61 us -> 0 us
  local copies, waits for them, and re-layouts: 16.4 us -> 11.8 us
  other arithmetic: 3.47 us -> 0.9 us
    pallas_call x1, Pallas kernels: 59.7 us -> 51.2 us  [attend(): pl.pallas_call(attend_kernel, out_shape=(jax.ShapeDtypeStruct((8, 32, 204...]
    dot_general x2 -> x0, matrix products: 4.61 us -> none  [the longest x1 3.03 us: local(): lax.dot_general(attended.reshape(8 * 128, 128), w_out, (((0,), (0,)), (()...]
    pallas_call x1, Pallas kernels: 93.2 us -> 95.8 us  [experts(): pl.pallas_call(expert_kernel, out_shape=jax.ShapeDtypeStruct((128, 2048),...]
    unnamed x19 -> x24, local copies, waits for them, and re-layouts: 11.6 us -> 11.8 us
where the time goes in v3:
time: 161 us; the launch traced here: 160 us
  Pallas kernels  147 us (91%)
  local copies, waits for them, and re-layouts  11.8 us (7%)
    pallas_call x1, Pallas kernels, experts(): pl.pallas_call(expert_kernel, out_shape=jax.ShapeDtypeStruct((128, 2048),...  95.8 us
    pallas_call x1, Pallas kernels, attend(): pl.pallas_call(attend_kernel, out_shape=(jax.ShapeDtypeStruct((8, 32, 204...  51.2 us
    unnamed x24, local copies, waits for them, and re-layouts  11.8 us

profile of v3, /device:TPU:1, one launch (start us, length us, event | category | flops | bytes accessed | tf_op | source)
XLA Modules:
  0.0 159.7 jit_solution(14912104817893583926)
XLA Ops:
  0.0 0.8 copy.14.ids_ref
  0.8 0.8 copy.15.rw_ref
  1.6 0.0 copy-start.1
  1.6 1.2 copy-done.1
  2.8 0.0 copy-start.2
  2.8 1.2 copy-done.2
  4.0 0.0 copy-start.4
  4.0 1.0 copy-done.4
  5.1 0.0 copy-start.5
  5.1 0.9 copy-done.5
  6.0 0.0 copy-start.6
  6.0 0.9 copy-done.6
  7.0 0.0 copy-start.7
  7.0 0.9 copy-done.7
  7.9 0.0 copy-start.8
  7.9 0.7 copy-done.8
  8.6 0.0 copy-start.9
  8.6 0.7 copy-done.9
  9.3 0.0 copy-start.10
  9.3 0.7 copy-done.10
  9.9 0.0 copy-start.3
  9.9 51.2 %attend.1 = (bf16[8,32,2048]{2,1,0:T(8,128)(2,1)S(1)}, bf16[8,32,128]{2,1,0:T(8,128)(2,1)S(1)}, bf16[128,2048]{1,0:T(8,128)(2,1)S(1)}, s32[128,1]{1,0:T(8,128)S(...) custom-call(f32[1,2]{1,0:T(1,128)S(1)} %bitcast.4, f32[1,128]{1,0:T(1,128)S(1)} %bitcast.5, ...), custom_call_target="tpu_custom_call" | custom-call | tf_op jit(solution)/shard_map/attend/pallas_call | solution.py:384
  61.1 0.0 copy-done.3
  61.1 0.0 copy-start
  61.1 1.9 %copy-done = bf16[3,2048,256]{2,1,0:T(8,128)(2,1)S(1)} copy-done((bf16[3,2048,256]{2,1,0:T(8,128)(2,1)S(1)}, bf16[3,2048,256]{2,1,0:T(8,128)(2,1)}, u32[]{:S(2)}) %copy-start) | copy-done | bytes 3145752
  63.0 95.8 %experts.1 = f32[128,2048]{1,0:T(8,128)S(1)} custom-call(bf16[8,32,2048]{2,1,0:T(8,128)(2,1)S(1)} %get-tuple-element.12.tok_in, bf16[8,32,128]{2,1,0:T(8,128)(2,1)S(1)} %get-tuple-element.13.meta_in, s32[128,1]{1,0:T(8,128)S(1)} %get-tuple-element.14.place_ref, bf16[4,2048,256]{2,1,0:T(8,128)(2,1)} %get-tuple-element.15.fg_ref, ...), custom_call_target="tpu_custom_call" | custom-call | tf_op jit(solution)/shard_map/experts/pallas_call | solution.py:660
  158.8 0.9 add_convert_fusion
Async XLA Ops:
  1.6 1.2 copy-start.1
  2.8 1.2 copy-start.2
  4.0 1.0 copy-start.4
  5.1 0.9 copy-start.5
  6.0 0.9 copy-start.6
  7.0 0.9 copy-start.7
  7.9 0.7 copy-start.8
  8.6 0.7 copy-start.9
  9.3 0.7 copy-start.10
  9.9 51.2 %copy-start.3 = (bf16[1,2048,256]{2,1,0:T(8,128)(2,1)S(1)}, bf16[1,2048,256]{2,1,0:T(8,128)(2,1)}, u32[]{:S(2)}) copy-start(bf16[1,2048,256]{2,1,0:T(8,128)(2,1)} %wd_ref.1) | copy-start | bytes 3145732
  61.1 1.9 %copy-start = (bf16[3,2048,256]{2,1,0:T(8,128)(2,1)S(1)}, bf16[3,2048,256]{2,1,0:T(8,128)(2,1)}, u32[]{:S(2)}) copy-start(bf16[3,2048,256]{2,1,0:T(8,128)(2,1)} %get-tuple-element.16.fu_ref) | copy-start | bytes 9437188

commit v4 on v3

--- a/solution.py
+++ b/solution.py
@@ -35,12 +35,13 @@
         source = self.places[m][quarter] if source is None else source
         self.copy(m, source, quarter, self.twin, self.x, 2 + quarter).start()
 
-    def begin(self, m, source):
+    def begin_near(self, m, source):
         @pl.when(self.home)
         def _():
             self.copy(m, source, 1, self.s, self.beside, 0).start()
             self.share(m, 0, source)
 
+    def begin_cross(self, m, source):
         @pl.when(self.away)
         def _():
             self.copy(m, source, 2, self.s, self.opposite, 0).start()
@@ -74,8 +75,8 @@
                 self.wait(m, quarter)
 
 
-def attend_kernel(lam_ref, gain_ref, q_in, k_in, v_in, wout_hbm, res_ref, ngain_ref, ids_ref, rw_ref, wg_ref, wu_ref,
-                  group_ref, facts_out, carried_ref, place_ref, fg_ref, fu_ref,
+def attend_kernel(lam_ref, gain_ref, q_in, k_in, v_in, wout_hbm, res_ref, ngain_ref, ids_ref, rw_ref, wg_ref, wu_ref, wd_ref,
+                  group_ref, facts_out, carried_ref, place_ref, fg_ref, fu_ref, fd_ref,
                   q_ref, v_ref, kbuf, vbuf, qbuf, qz, sbuf, ebuf, acc, mrun, att, o_ref, wout, facts,
                   ssem, rsem, qsem, osend, orecv, wsend, wrecv, lsem):
     s = lax.axis_index("sp")
@@ -110,8 +111,6 @@
         v_ref[b] = jnp.transpose(v_in[:, 128 * b:128 * (b + 1)])
     out_load = pltpu.make_async_copy(wout_hbm, wout, lsem.at[0])
     out_load.start()
-    own_loads = (pltpu.make_async_copy(wg_ref.at[0], fg_ref.at[0], lsem.at[1]),
-                 pltpu.make_async_copy(wu_ref.at[0], fu_ref.at[0], lsem.at[2]))
     pl.semaphore_wait(barrier, len(peers))
 
     def kslot(slot):
@@ -153,11 +152,12 @@
     start(pair_copy(own_k, own_v, mine, y1dev, 1))
     start(pair_copy(own_k, own_v, mine, y3dev, 2))
 
-    weights = WeightExchange(s, x, ([fg_ref.at[i] for i in range(4)], [fu_ref.at[i] for i in range(3)]), wsend, wrecv)
-    weights.begin(0, wg_ref.at[0])
-    weights.begin(1, wu_ref.at[0])
-    for own in own_loads:
-        pl.when(weights.home)(own.start)
+    weights = WeightExchange(s, x, ([fg_ref.at[i] for i in range(4)], [fu_ref.at[i] for i in range(3)],
+                                    [None, None, fd_ref, None]), wsend, wrecv)
+    for m, source in enumerate((wg_ref.at[0], wu_ref.at[0], wd_ref.at[0])):
+        weights.begin_cross(m, source)
+        if m < 2:
+            weights.begin_near(m, source)
 
     kbuf[mine // 2, pl.ds(pl.multiple_of(c * rows, rows), rows), :] = key_columns(zb)[...]
     vbuf[mine, pl.ds(0, 128), :] = v_ref[zb]
@@ -251,9 +251,6 @@
         @pl.when(i == 5)
         def _():
             weights.landed(1, 2)
-
-        @pl.when(i == 6)
-        def _():
             weights.landed(1, 1)
         j = i // 2
         gray = j + (j // 2) - 2 * (j // 2) * (j % 2)
@@ -297,6 +294,7 @@
             device_id={"sp": s, "tp": xx}, device_id_type=MESH))
         sends[-1].start()
     head_columns(head)[...] = att[x]
+    weights.landed(2, 2)
     weights.landed(0, 3)
     out_load.wait()
     for j in range(4):
@@ -330,10 +328,9 @@
     for copy in sends:
         copy.wait_send()
     qcopy.wait_send()
-    for own in own_loads:
-        pl.when(weights.home)(own.wait)
     weights.finish(0, wg_ref.at[0], (0, 1, 2, 3))
     weights.finish(1, wu_ref.at[0], (0, 1, 2))
+    weights.finish(2, wd_ref.at[0], (2,))
     for idx in range(15):
         a, b = pair_copy(own_k, own_v, mine, twin, idx)
         a.wait_send()
@@ -345,11 +342,13 @@
 
 
 def routing(z, ids_ref, rw_ref, facts, place_ref):
-    ids = ids_ref[...]
-    first, second = ids[:, 0:1], ids[:, 1:2]
-    both = jnp.concatenate([jnp.broadcast_to(first, (128, 128)), jnp.broadcast_to(second, (128, 128))], axis=1)
-    turned = jnp.transpose(both.astype(jnp.float32)).astype(jnp.int32)
-    first_row, second_row = turned[:128], turned[128:]
+    first_row, second_row = ids_ref[0:1, :], ids_ref[1:2, :]
+
+    def column(row):
+        return jnp.transpose(jnp.broadcast_to(row, (128, 128)))[:, 0:1]
+
+    first = column(first_row.astype(jnp.float32)).astype(jnp.int32)
+    second = column(second_row.astype(jnp.float32)).astype(jnp.int32)
     earlier = lax.broadcasted_iota(jnp.int32, (128, 128), 1) < lax.broadcasted_iota(jnp.int32, (128, 128), 0)
 
     def count(mask):
@@ -365,16 +364,16 @@
     place_ref[...] = turn * 32 + position
     row0 = ((first & 7) * 16 + slot0).astype(jnp.float32)
     row1 = ((second & 7) * 16 + slot1).astype(jnp.float32)
-    w0, w1 = rw_ref[:, 0:1], rw_ref[:, 1:2]
+    w0, w1 = column(rw_ref[0:1, :]), column(rw_ref[1:2, :])
     h0, h1 = w0.astype(jnp.bfloat16).astype(jnp.float32), w1.astype(jnp.bfloat16).astype(jnp.float32)
     lane = lax.broadcasted_iota(jnp.int32, (128, 128), 1)
     table = jnp.zeros((128, 128), jnp.float32)
-    for n, column in enumerate((row0, row1, h0, w0 - h0, h1, w1 - h1)):
-        table = jnp.where(lane == n, column, table)
+    for n, value in enumerate((row0, row1, h0, w0 - h0, h1, w1 - h1)):
+        table = jnp.where(lane == n, value, table)
     facts[...] = table.astype(jnp.bfloat16)
 
 
-def attend(queries, keys, values, lambdas, head_gain, w_out, residual_in, norm_gain, route_ids, route_weight, w_gate, w_up):
+def attend(queries, keys, values, lambdas, head_gain, w_out, residual_in, norm_gain, route_ids, route_weight, w_gate, w_up, w_down):
     rows = queries.shape[0]
     bf, f32 = jnp.bfloat16, jnp.float32
     tiles = 4 * rows // 256
@@ -385,9 +384,10 @@
         attend_kernel,
         out_shape=(jax.ShapeDtypeStruct((8, 32, 2048), bf), jax.ShapeDtypeStruct((8, 32, 128), bf),
                    jax.ShapeDtypeStruct((128, 2048), bf), jax.ShapeDtypeStruct((128, 1), jnp.int32),
-                   jax.ShapeDtypeStruct((4,) + w_gate.shape[1:], bf), jax.ShapeDtypeStruct((3,) + w_up.shape[1:], bf)),
-        in_specs=[pl.BlockSpec(memory_space=pltpu.SMEM), vm, vm, vm, vm, hbm, vm, vm, vm, vm, hbm, hbm],
-        out_specs=(vm, vm, vm, vm, vm, vm),
+                   jax.ShapeDtypeStruct((4,) + w_gate.shape[1:], bf), jax.ShapeDtypeStruct((3,) + w_up.shape[1:], bf),
+                   jax.ShapeDtypeStruct(w_down.shape[1:], bf)),
+        in_specs=[pl.BlockSpec(memory_space=pltpu.SMEM), vm, vm, vm, vm, hbm, vm, vm, vm, vm, hbm, hbm, hbm],
+        out_specs=(vm, vm, vm, vm, hbm, hbm, hbm),
         scratch_shapes=[
             pltpu.VMEM((2, 128, rows), bf),
             pltpu.VMEM((2, 128, rows), bf),
@@ -403,20 +403,20 @@
             pltpu.VMEM((128, 1024), bf),
             pltpu.VMEM((1024, 2048), bf),
             pltpu.VMEM((128, 128), bf),
-            dma((15, 2)), dma((16, 2)), dma((2,)), dma((7,)), dma((8,)), dma((2, 6)), dma((2, 4)), dma((3,)),
+            dma((15, 2)), dma((16, 2)), dma((2,)), dma((7,)), dma((8,)), dma((3, 6)), dma((3, 4)), dma((1,)),
         ],
         compiler_params=pltpu.CompilerParams(collective_id=1, has_side_effects=True,
-                                             vmem_limit_bytes=48 * 1024 * 1024),
+                                             vmem_limit_bytes=63 * 1024 * 1024),
         name="attend",
     )(lambdas.reshape(1, 2), head_gain.reshape(1, 128), queries, keys, values, w_out, residual_in,
-      norm_gain.reshape(1, -1), route_ids, route_weight, w_gate, w_up)
+      norm_gain.reshape(1, -1), jnp.transpose(route_ids), jnp.transpose(route_weight), w_gate, w_up, w_down)
 
 
 Z_STEPS = (0, 1, 7, 2, 6, 3, 5, 4)
 
 
-def expert_kernel(tok_in, meta_in, place_ref, fg_ref, fu_ref, wd_ref, o_ref,
-                  tok, meta, ex, er, ufar, wd, hb, yb, rb, cb, fin,
+def expert_kernel(tok_in, meta_in, place_ref, fg_ref, fu_ref, fd_ref, wg_ref, wu_ref, wd_ref, o_ref,
+                  tok, meta, ex, er, gw, uw, wd, hb, yb, rb, cb, fin,
                   tsend, trecv, msend, mrecv, esend, erecv, ysend, yrecv, fsend, frecv, wsem, dsend, drecv):
     s = lax.axis_index("sp")
     x = lax.axis_index("tp")
@@ -424,7 +424,7 @@
     y = (s // 2) % 4
     c = s % 2
     side = x // 2
-    weights = WeightExchange(s, x, ([None, None, None, ufar], [wd.at[i] for i in range(4)]), dsend, drecv)
+    weights = WeightExchange(s, x, ([None, None, None, uw.at[3]], [wd.at[i] for i in range(4)]), dsend, drecv)
     own_down = wd_ref.at[0]
 
     def z_device(step):
@@ -490,9 +490,31 @@
         for copy in token_copies(n):
             copy.start()
     weights.pass_on(0, fu_ref.at[2])
-    weights.begin(1, own_down)
-    own_load = pltpu.make_async_copy(own_down, wd.at[0], wsem.at[0])
-    pl.when(weights.home)(own_load.start)
+    weights.begin_near(1, own_down)
+    weights.pass_on(1, fd_ref)
+    far_load = pltpu.make_async_copy(fd_ref, wd.at[2], wsem.at[2, 1])
+    far_load.start()
+    own_load = pltpu.make_async_copy(own_down, wd.at[0], wsem.at[2, 0])
+
+    def load(m, source, q):
+        return pltpu.make_async_copy(source, (gw, uw)[m].at[q], wsem.at[m, q])
+
+    full_refs, own_refs = (fg_ref, fu_ref), (wg_ref, wu_ref)
+
+    @pl.when(weights.home)
+    def _():
+        own_load.start()
+        for m in range(2):
+            load(m, own_refs[m].at[0], 0).start()
+
+    @pl.when(weights.away)
+    def _():
+        for m in range(2):
+            load(m, full_refs[m].at[0], 0).start()
+
+    later_loads = [load(m, full_refs[m].at[q], q) for q in range(1, 4) for m in range(2) if q < 3 or m == 0]
+    for later in later_loads:
+        later.start()
 
     tok[0] = tok_in[0]
     meta[0] = meta_in[0]
@@ -527,7 +549,7 @@
             block = jnp.dot(even, tok[2 * p, :, here], preferred_element_type=jnp.float32)
             block += jnp.dot(odd, tok[2 * p + 1, :, here], preferred_element_type=jnp.float32)
             ex[p, :, :, here] = block.astype(jnp.bfloat16).reshape(8, 16, 512)
-        for k in (0, 1, 2, 3, 6, 7, 4, 5):
+        for k in (4, 2, 6, 5, 3, 7, 0, 1):
             when_remote_expert(k, lambda k=k: expert_copy(p, k).start())
 
         @pl.when(jnp.logical_not(other))
@@ -547,35 +569,40 @@
             yb.at[p, hub_number(h)], rb.at[p, my_expert], ysend.at[p, h], yrecv.at[p, my_expert],
             device_id={"sp": sp, "tp": tp}, device_id_type=MESH)
 
-    def hidden(half):
+    def hidden(p):
         def one_quarter(q, carry):
-            unit(q, fu_ref[q])
+            rows = er[p].reshape(128, 2048)
+            gate = jnp.dot(rows, gw[q], preferred_element_type=jnp.float32)
+            up = jnp.dot(rows, uw[q], preferred_element_type=jnp.float32)
+            hb[p, q] = (gate / (1.0 + jnp.exp(-gate)) * up).astype(jnp.bfloat16)
             return carry
 
-        def unit(q, up_weight):
-            rows = er[pl.ds(2 * half, 2)].reshape(256, 2048)
-            gate = jnp.dot(rows, fg_ref[q], preferred_element_type=jnp.float32)
-            up = jnp.dot(rows, up_weight, preferred_element_type=jnp.float32)
-            hb[q] = (gate / (1.0 + jnp.exp(-gate)) * up).astype(jnp.bfloat16)
-
-        lax.fori_loop(0, 3, one_quarter, 0)
-        if half == 0:
+        expert_rows_wait(p)
+        if p == 0:
+            for later in later_loads:
+                later.wait()
+            for m in range(2):
+                load(m, full_refs[m].at[0], 0).wait()
             weights.landed(0, 3)
             weights.finish(0, own_down, (3,))
-        unit(3, ufar[...])
-
-    def outputs(half):
-        for part in range(8):
-            here = pl.ds(part * 256, 256)
+        lax.fori_loop(0, 4, one_quarter, 0)
+
+    def outputs(p):
+        def one_part(part, carry):
+            here = pl.ds(pl.multiple_of(part * 256, 256), 256)
             total = None
             for q in range(4):
-                term = lax.dot_general(hb[q], wd[q, here, :], (((1,), (1,)), ((), ())),
+                term = lax.dot_general(hb[p, q], wd[q, here, :], (((1,), (1,)), ((), ())),
                                        preferred_element_type=jnp.float32)
                 total = term if total is None else total + term
-            yb[pl.ds(2 * half, 2), :, :, here] = total.astype(jnp.bfloat16).reshape(2, 8, 16, 256)
+            yb[p, :, :, here] = total.astype(jnp.bfloat16).reshape(8, 16, 256)
+            return carry
+
+        lax.fori_loop(0, 8, one_part, 0)
+        send_back(p)
 
     def send_back(p):
-        for h in (0, 1, 2, 3, 6, 7, 4, 5):
+        for h in (4, 2, 6, 5, 3, 7, 0, 1):
             when_remote_hub(h, lambda h=h: output_copy(p, h).start())
 
         @pl.when(jnp.logical_not(other))
@@ -609,28 +636,25 @@
 
     dispatch(0)
     dispatch(1)
-    weights.landed(1, 2)
-    weights.pass_on(1)
+    hidden(0)
     dispatch(2)
-    expert_rows_wait(0)
-    expert_rows_wait(1)
-    hidden(0)
+    weights.landed(1, 1)
+    hidden(1)
     dispatch(3)
     pl.when(weights.home)(own_load.wait)
-    weights.landed(1, 1)
+    far_load.wait()
     weights.landed(1, 3)
-    weights.finish(1, own_down, (0, 1, 2, 3))
+    weights.finish(1, own_down, (0, 1, 3))
     outputs(0)
-    send_back(0)
-    send_back(1)
-    expert_rows_wait(2)
-    expert_rows_wait(3)
-    hidden(1)
     outputs(1)
-    send_back(2)
-    send_back(3)
-    for p in range(4):
-        combine(p)
+    hidden(2)
+    outputs(2)
+    combine(0)
+    hidden(3)
+    outputs(3)
+    combine(1)
+    combine(2)
+    combine(3)
 
     for n in range(1, 8):
         final_copy(n).wait_recv()
@@ -652,7 +676,7 @@
             when_remote_hub(k, lambda k=k: output_copy(p, k).wait_send())
 
 
-def experts(grouped, facts, place, full_gate, full_up, w_down):
+def experts(grouped, facts, place, full_gate, full_up, down_cross, w_gate, w_up, w_down):
     bf, f32 = jnp.bfloat16, jnp.float32
     vm = pl.BlockSpec(memory_space=pltpu.VMEM)
     hbm = pl.BlockSpec(memory_space=pltpu.HBM)
@@ -660,35 +684,37 @@
     return pl.pallas_call(
         expert_kernel,
         out_shape=jax.ShapeDtypeStruct((128, 2048), f32),
-        in_specs=[vm, vm, vm, vm, vm, hbm],
+        in_specs=[vm, vm, vm, hbm, hbm, hbm, hbm, hbm, hbm],
         out_specs=vm,
         scratch_shapes=[
             pltpu.VMEM((8, 32, 2048), bf),
             pltpu.VMEM((8, 32, 128), bf),
             pltpu.VMEM((4, 8, 16, 2048), bf),
             pltpu.VMEM((4, 8, 16, 2048), bf),
-            pltpu.VMEM((2048, 256), bf),
             pltpu.VMEM((4, 2048, 256), bf),
-            pltpu.VMEM((4, 256, 256), bf),
+            pltpu.VMEM((4, 2048, 256), bf),
+            pltpu.VMEM((4, 2048, 256), bf),
+            pltpu.VMEM((4, 4, 128, 256), bf),
             pltpu.VMEM((4, 8, 16, 2048), bf),
             pltpu.VMEM((4, 8, 16, 2048), bf),
             pltpu.VMEM((8, 32, 2048), bf),
             pltpu.VMEM((8, 32, 2048), bf),
             dma((8,)), dma((8,)), dma((8,)), dma((8,)),
             dma((4, 8)), dma((4, 8)), dma((4, 8)), dma((4, 8)),
-            dma((8,)), dma((8,)), dma((1,)), dma((2, 6)), dma((2, 4)),
+            dma((8,)), dma((8,)), dma((3, 4)), dma((2, 6)), dma((2, 4)),
         ],
         compiler_params=pltpu.CompilerParams(collective_id=2, has_side_effects=True,
-                                             vmem_limit_bytes=46 * 1024 * 1024),
+                                             vmem_limit_bytes=60 * 1024 * 1024),
         name="experts",
-    )(grouped, facts, place, full_gate, full_up, w_down)
+    )(grouped, facts, place, full_gate, full_up, down_cross, w_gate, w_up, w_down)
 
 
 def local(queries, keys, values, lambdas, head_gain, w_out, residual_in, norm_gain,
           route_ids, route_weight, w_gate, w_up, w_down):
-    grouped, facts, carried, place, full_gate, full_up = attend(
-        queries, keys, values, lambdas, head_gain, w_out, residual_in, norm_gain, route_ids, route_weight, w_gate, w_up)
-    mixture = experts(grouped, facts, place, full_gate, full_up, w_down)
+    grouped, facts, carried, place, full_gate, full_up, down_cross = attend(
+        queries, keys, values, lambdas, head_gain, w_out, residual_in, norm_gain, route_ids, route_weight,
+        w_gate, w_up, w_down)
+    mixture = experts(grouped, facts, place, full_gate, full_up, down_cross, w_gate, w_up, w_down)
     return (carried.astype(jnp.float32) + mixture).astype(jnp.bfloat16)
 
 

time: 161 us -> 149 us (0.925)
  local copies, waits for them, and re-layouts: 11.8 us -> 0.01 us
    unnamed x24 -> x2, local copies, waits for them, and re-layouts: 11.8 us -> 0.01 us
where the time goes in v4:
time: 149 us
  Pallas kernels  146 us (98%)
  other arithmetic  2.13 us (1%)
    pallas_call x1, Pallas kernels, experts(): pl.pallas_call(expert_kernel, out_shape=jax.ShapeDtypeStruct((128, 2048),...  95.8 us
    pallas_call x1, Pallas kernels, attend(): pl.pallas_call(attend_kernel, out_shape=(jax.ShapeDtypeStruct((8, 32, 204...  50.6 us

profile of v4, /device:TPU:1, one launch (start us, length us, event | category | flops | bytes accessed | tf_op | source)
XLA Modules:
  0.0 148.6 jit_solution(10829701730670873604)
XLA Ops:
  0.0 50.6 %attend.1 = (bf16[8,32,2048]{2,1,0:T(8,128)(2,1)}, bf16[8,32,128]{2,1,0:T(8,128)(2,1)}, bf16[128,2048]{1,0:T(8,128)(2,1)}, s32[128,1]{1,0:T(8,128)}, bf16[4,2048...) custom-call(f32[1,2]{1,0:T(1,128)} %bitcast.8, f32[1,128]{1,0:T(1,128)} %bitcast.9, ...), custom_call_target="tpu_custom_call" | custom-call | tf_op jit(solution)/shard_map/attend/pallas_call | solution.py:383
  50.6 0.0 copy-start
  50.6 95.8 %experts.1 = f32[128,2048]{1,0:T(8,128)} custom-call(bf16[8,32,2048]{2,1,0:T(8,128)(2,1)} %get-tuple-element.13.tok_in, bf16[8,32,128]{2,1,0:T(8,128)(2,1)} %get-tuple-element.14.meta_in, s32[128,1]{1,0:T(8,128)} %get-tuple-element.15.place_ref, bf16[4,2048,256]{2,1,0:T(8,128)(2,1)} %get-tuple-element.16.fg_ref, ...), custom_call_target="tpu_custom_call" | custom-call | tf_op jit(solution)/shard_map/experts/pallas_call | solution.py:684
  146.4 0.0 copy-done
  146.4 2.1 %add_convert_fusion = bf16[128,2048]{1,0:T(8,128)(2,1)} fusion(f32[128,2048]{1,0:T(8,128)} %experts.1, bf16[128,2048]{1,0:T(8,128)(2,1)S(1)} %copy-done), kind=kLoop, calls=%fused_computation | loop fusion | flops 786432 | bytes 2097152 | tf_op jit(solution)/shard_map/convert_element_type | solution.py:718
Async XLA Ops:
  50.6 95.8 %copy-start = (bf16[128,2048]{1,0:T(8,128)(2,1)S(1)}, bf16[128,2048]{1,0:T(8,128)(2,1)}, u32[]{:S(2)}) copy-start(bf16[128,2048]{1,0:T(8,128)(2,1)} %get-tuple-element.12) | copy-start | bytes 1572868

commit v5 on v4

--- a/solution.py
+++ b/solution.py
@@ -222,15 +222,12 @@
         flip, yy = order[i]
         zz = zb + flip - 2 * zb * flip
         slot = slot_of(zz, yy, c)
-        wait_slot(slot)
-        if i == 1:
-            forward(slot, y1dev, 4)
-            forward(slot, y3dev, 5)
-        if i == 2:
-            forward(slot, y3dev, 8)
-        if i == 5:
-            forward(slot, y1dev, 12)
-        forward(slot, twin, {1: 6, 2: 7, 3: 9, 4: 10, 5: 11, 6: 13, 7: 14}[i])
+        there = {1: ((y1dev, 4), (y3dev, 5)), 2: ((y3dev, 8),), 5: ((y1dev, 12),)}.get(i, ())
+        there += ((twin, {1: 6, 2: 7, 3: 9, 4: 10, 5: 11, 6: 13, 7: 14}[i]),)
+        for half in range(2):
+            pair_copy(kslot(slot), vslot(slot), slot, twin, 0)[half].wait_recv()
+            for dest, idx in there:
+                pair_copy(kslot(slot), vslot(slot), slot, dest, idx)[half].start()
 
     def step(i, carry):
         @pl.when(i == 1)
@@ -486,7 +483,7 @@
                 pltpu.make_async_remote_copy(meta_in.at[n], meta.at[n], msend.at[n], mrecv.at[n],
                                              device_id=dest, device_id_type=MESH))
 
-    for n in range(1, 8):
+    for n in (7, 6, 5, 4, 3, 2, 1):
         for copy in token_copies(n):
             copy.start()
     weights.pass_on(0, fu_ref.at[2])
@@ -578,7 +575,7 @@
             return carry
 
         expert_rows_wait(p)
-        if p == 0:
+        if p == 3:
             for later in later_loads:
                 later.wait()
             for m in range(2):
@@ -634,27 +631,25 @@
             if n > 0:
                 final_copy(n).start()
 
-    dispatch(0)
-    dispatch(1)
-    hidden(0)
-    dispatch(2)
+    for p in (3, 2, 1, 0):
+        dispatch(p)
+    hidden(3)
     weights.landed(1, 1)
-    hidden(1)
-    dispatch(3)
+    hidden(2)
     pl.when(weights.home)(own_load.wait)
     far_load.wait()
     weights.landed(1, 3)
     weights.finish(1, own_down, (0, 1, 3))
+    outputs(3)
+    outputs(2)
+    hidden(1)
+    outputs(1)
+    combine(3)
+    hidden(0)
     outputs(0)
-    outputs(1)
-    hidden(2)
-    outputs(2)
+    combine(2)
+    combine(1)
     combine(0)
-    hidden(3)
-    outputs(3)
-    combine(1)
-    combine(2)
-    combine(3)
 
     for n in range(1, 8):
         final_copy(n).wait_recv()

time: 149 us -> 140 us (0.940)
  Pallas kernels: 146 us -> 138 us
    pallas_call x1, Pallas kernels: 95.8 us -> 87.3 us  [experts(): pl.pallas_call(expert_kernel, out_shape=jax.ShapeDtypeStruct((128, 2048),...]
where the time goes in v5:
time: 140 us
  Pallas kernels  138 us (99%)
  other arithmetic  2.13 us (2%)
    pallas_call x1, Pallas kernels, experts(): pl.pallas_call(expert_kernel, out_shape=jax.ShapeDtypeStruct((128, 2048),...  87.3 us
    pallas_call x1, Pallas kernels, attend(): pl.pallas_call(attend_kernel, out_shape=(jax.ShapeDtypeStruct((8, 32, 204...  50.8 us

profile of v5, /device:TPU:1, one launch (start us, length us, event | category | flops | bytes accessed | tf_op | source)
XLA Modules:
  0.0 140.3 jit_solution(16866558160682054317)
XLA Ops:
  0.0 50.8 %attend.1 = (bf16[8,32,2048]{2,1,0:T(8,128)(2,1)}, bf16[8,32,128]{2,1,0:T(8,128)(2,1)}, bf16[128,2048]{1,0:T(8,128)(2,1)}, s32[128,1]{1,0:T(8,128)}, bf16[4,2048...) custom-call(f32[1,2]{1,0:T(1,128)} %bitcast.8, f32[1,128]{1,0:T(1,128)} %bitcast.9, ...), custom_call_target="tpu_custom_call" | custom-call | tf_op jit(solution)/shard_map/attend/pallas_call | solution.py:380
  50.8 0.0 copy-start
  50.8 87.3 %experts.1 = f32[128,2048]{1,0:T(8,128)} custom-call(bf16[8,32,2048]{2,1,0:T(8,128)(2,1)} %get-tuple-element.13.tok_in, bf16[8,32,128]{2,1,0:T(8,128)(2,1)} %get-tuple-element.14.meta_in, s32[128,1]{1,0:T(8,128)} %get-tuple-element.15.place_ref, bf16[4,2048,256]{2,1,0:T(8,128)(2,1)} %get-tuple-element.16.fg_ref, ...), custom_call_target="tpu_custom_call" | custom-call | tf_op jit(solution)/shard_map/experts/pallas_call | solution.py:679
  138.1 0.0 copy-done
  138.2 2.1 %add_convert_fusion = bf16[128,2048]{1,0:T(8,128)(2,1)} fusion(f32[128,2048]{1,0:T(8,128)} %experts.1, bf16[128,2048]{1,0:T(8,128)(2,1)S(1)} %copy-done), kind=kLoop, calls=%fused_computation | loop fusion | flops 786432 | bytes 2097152 | tf_op jit(solution)/shard_map/convert_element_type | solution.py:713
Async XLA Ops:
  50.8 87.4 %copy-start = (bf16[128,2048]{1,0:T(8,128)(2,1)S(1)}, bf16[128,2048]{1,0:T(8,128)(2,1)}, u32[]{:S(2)}) copy-start(bf16[128,2048]{1,0:T(8,128)(2,1)} %get-tuple-element.12) | copy-start | bytes 1572868
